TPU v7x, 128 devices: a whole 4x4x4 slice. The times are simulated.
128 devices in a mesh: fs: 16 (over z, y), tp: 8 (over x, core).
Axes of the slice: x: 4, y: 4, z: 4, core: 2. Of those that a mesh axis runs over, the one named last changes fastest.
Arguments:
- tokens: bfloat16 [12288, 2048], P('fs', 'tp'), may hold values from -40 to 40
- gain_one: float32 [2048], P('tp'), may hold values from 0.1 to 1.9
- w_gate: float32 [2048, 3072], P('fs', 'tp'), may hold values from -0.125 to 0.125
- w_up: float32 [2048, 3072], P('fs', 'tp'), may hold values from -0.125 to 0.125
- w_down: float32 [3072, 2048], P('tp', 'fs'), may hold values from -0.109375 to 0.109375
- scale_gate: float32 [3072], P('tp'), may hold values from 0.5 to 2
- scale_up: float32 [3072], P('tp'), may hold values from 0.5 to 2
- scale_down: float32 [2048], P('tp'), may hold values from 0.5 to 2
- gain_mix: float32 [2048], P('tp'), may hold values from 0.1 to 1.9
- w_query: float32 [2048, 2048], P('fs', 'tp'), may hold values from -0.125 to 0.125
- w_key: float32 [2048, 2048], P('fs', 'tp'), may hold values from -0.125 to 0.125
- w_value: float32 [2048, 2048], P('fs', 'tp'), may hold values from -0.125 to 0.125
- w_outgate: float32 [2048, 2048], P('fs', 'tp'), may hold values from -0.125 to 0.125
- scale_query: float32 [2048], P('tp'), may hold values from 0.5 to 2
- scale_key: float32 [2048], P('tp'), may hold values from 0.5 to 2
- scale_value: float32 [2048], P('tp'), may hold values from 0.5 to 2
- scale_outgate: float32 [2048], P('tp'), may hold values from 0.5 to 2
- ret_gain: float32 [2048], P('tp'), may hold values from 0.1 to 1.9
- decay_rate: float32 [8], P('tp'), may hold values from 0 to 2
- w_mix: float32 [2048, 2048], P('tp', 'fs'), may hold values from -0.125 to 0.125
- scale_mix: float32 [2048], P('tp'), may hold values from 0.5 to 2
- gain_two: float32 [2048], P('tp'), may hold values from 0.1 to 1.9
Outputs:
- layer_out: bfloat16 [12288, 2048], P('fs', 'tp')
All inputs are finite; a program needn't handle non-finite values.
Results may differ from a plain program's by a relative error of at most 0.022.
Values may be sent and summed in bfloat16 or wider, within the bound.
A program may use at most 128 MiB of HBM per device.

v0:
```python
import jax
import jax.numpy as jnp
from jax import lax
from jax.sharding import PartitionSpec as P

D = 2048
LEN = 256
BLK = 128


EPS = 1e-06
HEAD_EPS = 0.1


def from_everyone(shard, axis):
    copies = jnp.broadcast_to(shard, (lax.axis_size(axis), *shard.shape))
    return lax.all_to_all(copies, axis, split_axis=0, concat_axis=0, tiled=True)


def taken_together(shard, axis):
    return from_everyone(shard, axis).sum(axis=0)


def in_blocks(shard, dim, length):
    shape = shard.shape
    blocks = shard.reshape(*shape[:dim], length, shape[dim] // length, *shape[dim + 1 :])
    return jnp.moveaxis(blocks, dim, 0)


def sent_and_summed(shard, axis, dim):
    length = lax.axis_size(axis)
    blocks = lax.all_to_all(in_blocks(shard, dim, length), axis, 0, 0, tiled=True)
    return jnp.sum(blocks.astype(jnp.float32), axis=0)


def side_by_side(arrays, axis, dim, along):
    widths = [a.shape[along] for a in arrays]
    both = jnp.concatenate(arrays, axis=along)
    out = lax.all_gather(both, axis, axis=dim, tiled=True)
    return tuple(jnp.split(out, [sum(widths[:k]) for k in range(1, len(widths))], axis=along))


def laid_out(blocks, dim):
    blocks = jnp.moveaxis(blocks, 0, dim)
    shape = blocks.shape
    return blocks.reshape(*shape[:dim], shape[dim] * shape[dim + 1], *shape[dim + 2 :])


def gathered_copies(shard, axis, dim):
    return laid_out(from_everyone(shard, axis), dim)


def rotate_pairs(values):
    paired = values.reshape(values.shape[:-1] + (values.shape[-1] // 2, 2))
    return jnp.stack((-paired[..., 1], paired[..., 0]), axis=-1).reshape(values.shape)


def retain(query_rows, key_rows, value_rows, decay_rate, length, block):
    total_rows = query_rows.shape[0]
    heads = decay_rate.shape[0]
    head_size = query_rows.shape[1] // heads
    sequences = total_rows // length
    nblocks = length // block

    def split_heads(values):
        return values.astype(jnp.float32).reshape(sequences, length, heads, head_size)

    freq = 1.0 / 10000.0 ** jnp.linspace(0.0, 1.0, head_size // 2, dtype=jnp.float32)
    freq = jnp.repeat(freq, 2)
    angles = jnp.arange(length, dtype=jnp.float32)[:, None] * freq[None, :]
    sines = jnp.sin(angles)[None, :, None, :]
    cosines = jnp.cos(angles)[None, :, None, :]
    queries = split_heads(query_rows)
    queries = queries * cosines + rotate_pairs(queries) * sines
    keys_all = split_heads(key_rows) * head_size ** (-0.5)
    keys_all = keys_all * cosines + rotate_pairs(keys_all) * sines
    values_all = split_heads(value_rows)
    log_decay = -decay_rate
    offsets = jnp.arange(block, dtype=jnp.float32)
    distance = offsets[:, None] - offsets[None, :]
    inside = jnp.where(
        distance >= 0, jnp.exp(log_decay[:, None, None] * jnp.maximum(distance, 0.0)), 0.0
    )
    query_decay = jnp.exp(log_decay[None, :] * (offsets[:, None] + 1.0))
    key_decay = jnp.exp(log_decay[None, :] * (block - 1.0 - offsets[:, None]))
    block_decay = jnp.exp(log_decay * block)

    def to_blocks(values):
        return jnp.moveaxis(values.reshape(sequences, nblocks, block, heads, head_size), 1, 0)

    def advance(carried, pieces):
        query_blk, key_blk, value_blk = pieces
        scores = jnp.einsum("snhd,smhd->shnm", query_blk, key_blk) * inside
        within = jnp.einsum("shnm,smhe->snhe", scores, value_blk)
        across = jnp.einsum("snhd,shde->snhe", query_blk, carried) * query_decay[None, :, :, None]
        weighted = key_blk * key_decay[None, :, :, None]
        carried = carried * block_decay[None, :, None, None] + jnp.einsum(
            "smhd,smhe->shde", weighted, value_blk
        )
        return (carried, within + across)

    initial = jnp.zeros((sequences, heads, head_size, head_size), jnp.float32)
    _, results = lax.scan(
        advance, initial, (to_blocks(queries), to_blocks(keys_all), to_blocks(values_all))
    )
    results = jnp.moveaxis(results, 0, 1).reshape(sequences, length, heads, head_size)
    results = results * lax.rsqrt(jnp.mean(results * results, axis=-1, keepdims=True) + HEAD_EPS)
    return results.reshape(total_rows, heads * head_size)


def normed_rows(hidden_in, norm_gain):
    widened = hidden_in.astype(jnp.float32)
    totals = taken_together(jnp.sum(widened * widened, axis=1), "tp")
    scaled = widened * lax.rsqrt(totals / D + EPS)[:, None] * norm_gain
    return lax.all_gather(scaled.astype(jnp.bfloat16), "tp", axis=1, tiled=True)


def summed_share(partial_value):
    rounded = lax.optimization_barrier(partial_value.astype(jnp.bfloat16))
    return sent_and_summed(rounded.astype(jnp.float32).astype(jnp.bfloat16), "tp", 1)


def ffn_gathered(features, gate_low, up_low, down_low, scale_gate, scale_up):
    pieces = side_by_side((gate_low, up_low), "fs", 0, 1)
    gate_add = jnp.dot(features, pieces[0], preferred_element_type=jnp.float32)
    up_add = jnp.dot(features, pieces[1], preferred_element_type=jnp.float32)
    hidden = (jax.nn.silu(gate_add * scale_gate) * (up_add * scale_up)).astype(jnp.bfloat16)
    return jnp.dot(hidden, gathered_copies(down_low, "fs", 1), preferred_element_type=jnp.float32)


def per_device(
    tokens,
    gain_one,
    w_gate,
    w_up,
    w_down,
    scale_gate,
    scale_up,
    scale_down,
    gain_mix,
    w_query,
    w_key,
    w_value,
    w_outgate,
    scale_query,
    scale_key,
    scale_value,
    scale_outgate,
    ret_gain,
    decay_rate,
    w_mix,
    scale_mix,
    gain_two,
):
    norm_one, norm_mix, norm_two, down_cols, mix_cols = (
        gain_one,
        gain_mix,
        gain_two,
        scale_down,
        scale_mix,
    )
    gate_low = w_gate.astype(jnp.bfloat16)
    up_low = w_up.astype(jnp.bfloat16)
    down_low = w_down.astype(jnp.bfloat16)
    ffn_one = ffn_gathered(
        normed_rows(tokens, norm_one), gate_low, up_low, down_low, scale_gate, scale_up
    )
    first = (tokens.astype(jnp.float32) + 0.5 * summed_share(ffn_one) * down_cols).astype(
        jnp.bfloat16
    )
    features = normed_rows(first, norm_mix)
    pieces = side_by_side(
        (
            w_query.astype(jnp.bfloat16),
            w_key.astype(jnp.bfloat16),
            w_value.astype(jnp.bfloat16),
            w_outgate.astype(jnp.bfloat16),
        ),
        "fs",
        0,
        1,
    )
    query_pre, key_pre, value_pre, outgate_pre = tuple(
        (jnp.dot(features, piece, preferred_element_type=jnp.float32) for piece in pieces)
    )
    query_rows = (query_pre * scale_query).astype(jnp.bfloat16)
    key_rows = (key_pre * scale_key).astype(jnp.bfloat16)
    value_rows = (value_pre * scale_value).astype(jnp.bfloat16)
    outgate_rows = (outgate_pre * scale_outgate).astype(jnp.bfloat16)
    retained = retain(query_rows, key_rows, value_rows, decay_rate, LEN, BLK)
    mixed = (retained * ret_gain * jax.nn.silu(outgate_rows.astype(jnp.float32))).astype(
        jnp.bfloat16
    )
    mix_partial = jnp.dot(
        mixed,
        gathered_copies(w_mix.astype(jnp.bfloat16), "fs", 1),
        preferred_element_type=jnp.float32,
    )
    second = (first.astype(jnp.float32) + summed_share(mix_partial) * mix_cols).astype(jnp.bfloat16)
    ffn_two = ffn_gathered(
        normed_rows(second, norm_two), gate_low, up_low, down_low, scale_gate, scale_up
    )
    result = (second.astype(jnp.float32) + 0.5 * summed_share(ffn_two) * down_cols).astype(
        jnp.bfloat16
    )
    return result


def solution(mesh):
    return jax.shard_map(
        per_device,
        mesh=mesh,
        in_specs=(
            P("fs", "tp"),
            P("tp"),
            P("fs", "tp"),
            P("fs", "tp"),
            P("tp", "fs"),
            P("tp"),
            P("tp"),
            P("tp"),
            P("tp"),
            P("fs", "tp"),
            P("fs", "tp"),
            P("fs", "tp"),
            P("fs", "tp"),
            P("tp"),
            P("tp"),
            P("tp"),
            P("tp"),
            P("tp"),
            P("tp"),
            P("tp", "fs"),
            P("tp"),
            P("tp"),
        ),
        out_specs=P("fs", "tp"),
        check_vma=False,
    )
```

profile of v0, /device:TPU:0, one launch (start us, length us, event | category | flops | bytes accessed | tf_op | source)
XLA Modules:
  0.0 379.6 jit_solution(7782225091500418627)
XLA Ops:
  7.9 9.6 %all_to_all.44 = f32[8,1,768]{2,1,0:T(1,128)S(1)} all-to-all(f32[8,1,768]{2,1,0:T(1,128)S(1)} %broadcast_in_dim.23), channel_id=1, replica_groups=mesh['fs'=16,'tp'=8] {'tp'}, dimensions={0} | all-to-all | bytes 49152 | tf_op jit(solution)/shard_map/all_to_all | solution.py:17
  17.5 1.9 fusion.54
  25.5 8.0 %all-to-all-start.1 = ((bf16[16,384,128]{1,2,0:T(8,128)(2,1)}), bf16[16,384,128]{1,2,0:T(8,128)(2,1)S(1)}, u32[]{:S(2)}, u32[]{:S(2)}) async-start(bf16[16,384,128]{1,2,0:T(8,128)(2,1)} %broadcast_in_dim.24), calls=%async_computation.1 | async-start | bytes 3145728 | tf_op jit(solution)/shard_map/all_to_all | solution.py:17
  33.5 17.7 %all-gather.6.cloned.1.call-done = bf16[768,2048]{1,0:T(8,128)(2,1)} async-done(((bf16[768,256]{1,0:T(8,128)(2,1)}), bf16[768,2048]{1,0:T(8,128)(2,1)}) %all-gather.6.cloned.1.call-update) | async-done | bytes 3145744 | tf_op jit(solution)/shard_map/all_gather | solution.py:115
  51.2 51.1 %all-gather.8.cloned.1.call-done = bf16[2048,768]{1,0:T(8,128)(2,1)} async-done(((bf16[128,768]{1,0:T(8,128)(2,1)}), bf16[2048,768]{1,0:T(8,128)(2,1)}) %all-gather.8.cloned.1.call-update) | async-done | bytes 3145744 | tf_op jit(solution)/shard_map/all_gather | solution.py:39
  102.3 5.2 %convolution_multiply_fusion.4 = f32[768,384]{1,0:T(8,128)} fusion(bf16[768,2048]{1,0:T(8,128)(2,1)} %all-gather.6.cloned.1.call-done, bf16[2048,768]{1,0:T(8,128)(2,1)} %all-gather.8.cloned.1.call-done, f32[384]{0:T(512)S(1)} %copy-done.21), kind=kOutput, calls=%fused_computation.47 | convolution fusion | flops 1208254464 | bytes 5899776 | tf_op jit(solution)/shard_map/dot_general | solution.py:125
  108.7 6.7 %convolution_convert_fusion.2 = bf16[768,2048]{1,0:T(8,128)(2,1)S(1)} fusion(bf16[384,2048]{0,1:T(8,128)(2,1)} %bitcast.163, bf16[768,2048]{1,0:T(8,128)(2,1)} %all-gather.6.cloned.1.call-done, bf16[2048,768]{1,0:T(8,128)(2,1)} %all-gather.8.cloned.1.call-done, f32[768,384]{1,0:T(8,128)} %convolution_multiply_fusion.4, f32[384]{0:T(512)S(1)} %copy-done.22), kind=kOutput, calls=%fused_computation.38 | convolution fusion | flops 2419556352 | bytes 10618368 | tf_op jit(solution)/shard_map/dot_general | solution.py:128
  115.3 2.0 copy.141
  117.3 4.4 %all-to-all-start.2 = ((bf16[8,768,256]{2,1,0:T(8,128)(2,1)}), bf16[8,768,256]{2,1,0:T(8,128)(2,1)S(1)}, u32[]{:S(2)}, u32[]{:S(2)}) async-start(bf16[8,768,256]{2,1,0:T(8,128)(2,1)} %bitcast.116), calls=%async_computation.2 | async-start | bytes 6291456 | tf_op jit(solution)/shard_map/all_to_all | solution.py:32
  121.8 38.3 %all-to-all-done.2 = bf16[8,768,256]{2,1,0:T(8,128)(2,1)S(1)} async-done(((bf16[8,768,256]{2,1,0:T(8,128)(2,1)}), bf16[8,768,256]{2,1,0:T(8,128)(2,1)S(1)}, u32[]{:S(2)}, u32[]{:S(2)}) %all-to-all-start.2) | async-done | bytes 3145760 | tf_op jit(solution)/shard_map/all_to_all | solution.py:32
  160.8 7.8 %all_to_all.45 = f32[8,1,768]{2,1,0:T(1,128)S(1)} all-to-all(f32[8,1,768]{2,1,0:T(1,128)S(1)} %broadcast_in_dim.27), channel_id=1, replica_groups=mesh['fs'=16,'tp'=8] {'tp'}, dimensions={0} | all-to-all | bytes 49152 | tf_op jit(solution)/shard_map/all_to_all | solution.py:17
  171.7 4.4 %all-to-all-start.4 = ((bf16[16,256,128]{1,2,0:T(8,128)(2,1)}), bf16[16,256,128]{1,2,0:T(8,128)(2,1)}, u32[]{:S(2)}, u32[]{:S(2)}) async-start(bf16[16,256,128]{1,2,0:T(8,128)(2,1)} %broadcast_in_dim.31), calls=%async_computation.4 | async-start | bytes 2097152 | tf_op jit(solution)/shard_map/all_to_all | solution.py:17
  177.3 8.5 %multiply_cosine_fusion = (f32[2,128,256]{1,0,2:T(2,128)}, f32[2,128,256]{1,0,2:T(2,128)}, f32[2,128,256]{1,0,2:T(2,128)}) fusion(f32[2,128]{1,0:T(2,128)S(1)} %multiply_add_fusion, f32[256]{0:T(256)S(1)} %mul.470), kind=kLoop, calls=%fused_computation.107 | loop fusion | flops 327680 | bytes 788480 | tf_op jit(solution)/shard_map/cos | solution.py:72
  185.9 11.7 %all-gather.10.cloned.1.call-done = bf16[768,2048]{1,0:T(8,128)(2,1)} async-done(((bf16[768,256]{1,0:T(8,128)(2,1)}), bf16[768,2048]{1,0:T(8,128)(2,1)}) %all-gather.10.cloned.1.call-update) | async-done | bytes 3145744 | tf_op jit(solution)/shard_map/all_gather | solution.py:115
  197.6 4.1 %broadcast_multiply_fusion = (f32[768,256]{1,0:T(8,128)S(1)}, f32[768,256]{1,0:T(8,128)}) fusion(f32[256]{0:T(256)S(1)} %copy-done.24, bf16[768,2048]{1,0:T(8,128)(2,1)} %all-gather.10.cloned.1.call-done, bf16[2048,1024]{1,0:T(8,128)(2,1)} %all-gather.12.cloned.1.call-done), kind=kOutput, calls=%fused_computation.106 | convolution fusion | flops 806092800 | bytes 5768192 | tf_op jit(solution)/shard_map/dot_general | solution.py:184
  202.9 1.7 copy.109
  204.6 2.2 fusion.41
  208.0 1.7 copy.113
  212.1 3.3 fusion.39
  215.6 1.9 add_bitcast_fusion
  217.4 8.8 %while.15 = (s32[]{:T(128)}, f32[3,1,256,256]{3,2,0,1:T(8,128)S(1)}, f32[2,3,128,1,256]{2,4,1,3,0:T(8,128)}, f32[1]{0:T(128)}, f32[2,3,128,1,256]{2,0,3,4,1:T(2,...) while((s32[]{:T(128)}, ...), condition=%wide.region_6.7_spmd.clone.clone.clone, body=%wide.region_5.6_spmd.clone.clone.clone.sunk | while | flops 152257024 | bytes 7998088 | solution.py:103
  217.4 2.0 constant_dynamic-slice_fusion.3
  221.7 1.9 constant_dynamic-slice_fusion.3
  226.2 1.4 copy.116
  228.9 3.2 fusion.66
  232.1 2.2 convolution_convert_fusion.1
  234.6 42.2 %all_to_all.46 = bf16[8,768,256]{2,1,0:T(8,128)(2,1)S(1)} all-to-all(bf16[8,768,256]{2,1,0:T(8,128)(2,1)S(1)} %bitcast.155), channel_id=1, replica_groups=mesh['fs'=16,'tp'=8] {'tp'}, dimensions={0} | all-to-all | bytes 6291456 | tf_op jit(solution)/shard_map/all_to_all | solution.py:32
  278.0 7.8 %all_to_all.47 = f32[8,1,768]{2,1,0:T(1,128)S(1)} all-to-all(f32[8,1,768]{2,1,0:T(1,128)S(1)} %broadcast_in_dim.32), channel_id=1, replica_groups=mesh['fs'=16,'tp'=8] {'tp'}, dimensions={0} | all-to-all | bytes 49152 | tf_op jit(solution)/shard_map/all_to_all | solution.py:17
  286.8 30.6 %all-gather.14.cloned.1.call-done = bf16[768,2048]{1,0:T(8,128)(2,1)} async-done(((bf16[768,256]{1,0:T(8,128)(2,1)}), bf16[768,2048]{1,0:T(8,128)(2,1)}) %all-gather.14.cloned.1.call-update) | async-done | bytes 3145744 | tf_op jit(solution)/shard_map/all_gather | solution.py:115
  317.4 5.3 %convolution_multiply_fusion.2 = f32[768,384]{1,0:T(8,128)} fusion(bf16[768,2048]{1,0:T(8,128)(2,1)} %all-gather.14.cloned.1.call-done, bf16[2048,768]{1,0:T(8,128)(2,1)} %all-gather.8.cloned.1.call-done, f32[384]{0:T(512)S(1)} %copy-done.21), kind=kOutput, calls=%fused_computation.44 | convolution fusion | flops 1208254464 | bytes 5899776 | tf_op jit(solution)/shard_map/dot_general | solution.py:125
  322.7 6.6 %convolution_convert_fusion = bf16[768,2048]{1,0:T(8,128)(2,1)S(1)} fusion(bf16[384,2048]{0,1:T(8,128)(2,1)} %bitcast.164, bf16[768,2048]{1,0:T(8,128)(2,1)} %all-gather.14.cloned.1.call-done, bf16[2048,768]{1,0:T(8,128)(2,1)} %all-gather.8.cloned.1.call-done, f32[768,384]{1,0:T(8,128)} %convolution_multiply_fusion.2, f32[384]{0:T(512)S(1)} %copy-done.23), kind=kOutput, calls=%fused_computation.36 | convolution fusion | flops 2419556352 | bytes 10618368 | tf_op jit(solution)/shard_map/dot_general | solution.py:128
  329.5 42.2 %all_to_all.48 = bf16[8,768,256]{2,1,0:T(8,128)(2,1)S(1)} all-to-all(bf16[8,768,256]{2,1,0:T(8,128)(2,1)S(1)} %bitcast.156), channel_id=1, replica_groups=mesh['fs'=16,'tp'=8] {'tp'}, dimensions={0} | all-to-all | bytes 6291456 | tf_op jit(solution)/shard_map/all_to_all | solution.py:32
  (140 shorter events, 27.2 us)
Async XLA Ops:
  6.5 16.6 %copy-start.13 = (f32[128,256]{1,0:T(8,128)S(1)}, f32[128,256]{1,0:T(8,128)}, u32[]{:S(2)}) copy-start(f32[128,256]{1,0:T(8,128)} %param.34) | copy-start | bytes 393220
  6.5 16.6 %copy-start.14 = (f32[128,256]{1,0:T(8,128)S(1)}, f32[128,256]{1,0:T(8,128)}, u32[]{:S(2)}) copy-start(f32[128,256]{1,0:T(8,128)} %param.35) | copy-start | bytes 393220
  6.5 16.6 %copy-start.15 = (f32[128,256]{1,0:T(8,128)S(1)}, f32[128,256]{1,0:T(8,128)}, u32[]{:S(2)}) copy-start(f32[128,256]{1,0:T(8,128)} %param.36) | copy-start | bytes 393220
  6.5 17.4 %copy-start.12 = (f32[384,128]{1,0:T(8,128)S(1)}, f32[384,128]{1,0:T(8,128)}, u32[]{:S(2)}) copy-start(f32[384,128]{1,0:T(8,128)} %param.28) | copy-start | bytes 589828
  6.5 44.7 %all-gather.6.cloned.1.call-start = ((), (), s32[]{:S(2)}) async-start(), calls=%async_computation.8 | async-start | bytes 3538944 | tf_op jit(solution)/shard_map/all_gather | solution.py:115
  19.5 82.8 %all-gather.8.cloned.1.call-start = ((), (), s32[]{:S(2)}) async-start(), calls=%async_computation.9 | async-start | bytes 3342336 | tf_op jit(solution)/shard_map/all_gather | solution.py:39
  22.1 163.8 %all-gather.12.cloned.1.call-start = ((), (), s32[]{:S(2)}) async-start(), calls=%async_computation.11 | async-start | bytes 4456448 | tf_op jit(solution)/shard_map/all_gather | solution.py:39
  23.2 79.1 %copy-start.21 = (f32[384]{0:T(512)S(1)}, f32[384]{0:T(512)}, u32[]{:S(2)}) copy-start(f32[384]{0:T(512)} %param.29) | copy-start | bytes 4612
  25.5 82.1 %all-to-all-start.1 = ((bf16[16,384,128]{1,2,0:T(8,128)(2,1)}), bf16[16,384,128]{1,2,0:T(8,128)(2,1)S(1)}, u32[]{:S(2)}, u32[]{:S(2)}) async-start(bf16[16,384,128]{1,2,0:T(8,128)(2,1)} %broadcast_in_dim.24), calls=%async_computation.1 | async-start | bytes 3145728 | tf_op jit(solution)/shard_map/all_to_all | solution.py:17
  33.5 75.2 %copy-start.22 = (f32[384]{0:T(512)S(1)}, f32[384]{0:T(512)}, u32[]{:S(2)}) copy-start(f32[384]{0:T(512)} %param.30) | copy-start | bytes 4612
  117.3 4.5 %copy-start.18 = (f32[256]{0:T(256)S(1)}, f32[256]{0:T(256)}, u32[]{:S(2)}) copy-start(f32[256]{0:T(256)} %param.31) | copy-start | bytes 3076
  117.3 42.8 %all-to-all-start.2 = ((bf16[8,768,256]{2,1,0:T(8,128)(2,1)}), bf16[8,768,256]{2,1,0:T(8,128)(2,1)S(1)}, u32[]{:S(2)}, u32[]{:S(2)}) async-start(bf16[8,768,256]{2,1,0:T(8,128)(2,1)} %bitcast.116), calls=%async_computation.2 | async-start | bytes 6291456 | tf_op jit(solution)/shard_map/all_to_all | solution.py:32
  121.7 38.8 %copy-start = (bf16[768,256]{1,0:T(8,128)(2,1)S(1)}, bf16[768,256]{1,0:T(8,128)(2,1)}, u32[]{:S(2)}) copy-start(bf16[768,256]{1,0:T(8,128)(2,1)} %param.24) | copy-start | bytes 1179652
  121.7 46.9 %copy-start.16 = (f32[256]{0:T(256)S(1)}, f32[256]{0:T(256)}, u32[]{:S(2)}) copy-start(f32[256]{0:T(256)} %param.32) | copy-start | bytes 3076
  121.7 75.9 %all-gather.10.cloned.1.call-start = ((), (), s32[]{:S(2)}) async-start(), calls=%async_computation.10 | async-start | bytes 3538944 | tf_op jit(solution)/shard_map/all_gather | solution.py:115
  160.8 15.3 %copy-start.1 = (bf16[768,256]{1,0:T(8,128)(2,1)}, bf16[768,256]{1,0:T(8,128)(2,1)S(1)}, u32[]{:S(2)}) copy-start(bf16[768,256]{1,0:T(8,128)(2,1)S(1)} %get-tuple-element.210) | copy-start | bytes 1179652
  160.8 36.8 %copy-start.24 = (f32[256]{0:T(256)S(1)}, f32[256]{0:T(256)}, u32[]{:S(2)}) copy-start(f32[256]{0:T(256)} %param.38) | copy-start | bytes 3076
  171.7 60.5 %all-to-all-start.4 = ((bf16[16,256,128]{1,2,0:T(8,128)(2,1)}), bf16[16,256,128]{1,2,0:T(8,128)(2,1)}, u32[]{:S(2)}, u32[]{:S(2)}) async-start(bf16[16,256,128]{1,2,0:T(8,128)(2,1)} %broadcast_in_dim.31), calls=%async_computation.4 | async-start | bytes 2097152 | tf_op jit(solution)/shard_map/all_to_all | solution.py:17
  176.1 141.4 %all-gather.14.cloned.1.call-start = ((), (), s32[]{:S(2)}) async-start(), calls=%async_computation.12 | async-start | bytes 3538944 | tf_op jit(solution)/shard_map/all_gather | solution.py:115
  207.5 2.2 copy-start.11
  207.7 4.3 %copy-start.26 = (f32[256]{0:T(256)S(1)}, f32[256]{0:T(256)}, u32[]{:S(2)}) copy-start(f32[256]{0:T(256)} %param.39) | copy-start | bytes 3076
  212.1 3.4 copy-start.3
  212.1 3.4 copy-start.4
  212.1 3.4 copy-start.5
  212.1 3.4 copy-start.6
  212.1 3.4 copy-start.8
  212.1 3.4 copy-start.9
  212.1 3.4 copy-start.10
  217.4 11.5 %copy-start.27 = (f32[256]{0:T(256)S(1)}, f32[256]{0:T(256)}, u32[]{:S(2)}) copy-start(f32[256]{0:T(256)} %param.40) | copy-start | bytes 3076
  217.4 11.5 %copy-start.28 = (f32[256]{0:T(256)S(1)}, f32[256]{0:T(256)}, u32[]{:S(2)}) copy-start(f32[256]{0:T(256)} %param.41) | copy-start | bytes 3076
  276.8 9.0 %copy-start.17 = (f32[256]{0:T(256)S(1)}, f32[256]{0:T(256)}, u32[]{:S(2)}) copy-start(f32[256]{0:T(256)} %param.45) | copy-start | bytes 3076
  286.8 35.9 %copy-start.23 = (f32[384]{0:T(512)S(1)}, f32[384]{0:T(512)}, u32[]{:S(2)}) copy-start(f32[384]{0:T(512)} %param.30) | copy-start | bytes 4612
  (5 other events, 7.5 us)
Sparse Core Ops, SparseCore 0:
  19.6 31.5 all-gather.5
  53.3 48.9 all-gather.7
  104.4 50.1 all-gather.11
  169.7 27.8 all-gather.9
  286.9 30.4 all-gather.13
where the time goes:
time: 381 us; the launch traced here: 380 us
  waiting for transfers between devices  150 us (39%)
  blocking collectives  110 us (29%)
  matrix products  42.7 us (11%)
  other arithmetic  25.7 us (7%)
  local copies, waits for them, and re-layouts  20.2 us (5%)
  starting transfers between devices  17.2 us (5%)
  between operations  14.5 us (4%)
    all_to_all x2, blocking collectives, sent_and_summed(): lax.all_to_all(in_blocks(shard, dim, length), axis, 0, 0, tiled=True)  84.4 us
    all_gather x3, waiting for transfers between devices, normed_rows(): return lax.all_gather(scaled.astype(jnp.bfloat16), 'tp', axis=1, tiled=True)  60 us
    all_gather x2, waiting for transfers between devices, side_by_side(): out = lax.all_gather(both, axis, axis=dim, tiled=True)  51.1 us
    all_to_all x1, waiting for transfers between devices, sent_and_summed(): lax.all_to_all(in_blocks(shard, dim, length), axis, 0, 0, tiled=True)  38.3 us
    all_to_all x3, blocking collectives, from_everyone(): return lax.all_to_all(copies, axis, split_axis=0, concat_axis=0, tiled=True)  25.1 us
    dot_general x2, matrix products, ffn_gathered(): jnp.dot(hidden, gathered_copies(down_low, 'fs', 1), preferred_element_typ...  13.3 us
    dot_general x4, matrix products, per_device(): jnp.dot(features, piece, preferred_element_type=jnp.float32)  12.8 us
    all_to_all x2, starting transfers between devices, from_everyone(): return lax.all_to_all(copies, axis, split_axis=0, concat_axis=0, tiled=True)  12.4 us
  transfers between devices with their start and end apart: 8, of which 5 were waited for; matrix products, arithmetic and copies ran while one was open for 17% of the time, Pallas kernels for 0%

commit v1 on v0

v1 whole, which is shorter than its diff:
```python
import functools

import jax
import jax.numpy as jnp
import numpy as np
from jax import lax
from jax.experimental import pallas as pl
from jax.experimental.pallas import tpu as pltpu
from jax.sharding import PartitionSpec as P

MESH = pl.DeviceIdType.MESH
BF16 = jnp.bfloat16
F32 = jnp.float32

D = 2048
LEN = 256
ROWS = 256
CHUNKS = 3
EPS = 1e-06
HEAD_EPS = 0.1
GROUPS = ("gu", "dn", "qk", "mx")
PIECE_ROWS = {"gu": 128, "dn": 384, "qk": 128, "mx": 256}
PIECE_BYTES = {"gu": 196608, "dn": 98304, "qk": 262144, "mx": 65536}
BLOCK = 131072


class Step:
    def __init__(self, run, waits=(), sends=(), needs=(), gives=None, cost=0.1, rank=1.0):
        self.run, self.waits, self.sends = run, waits, sends
        self.needs, self.gives, self.cost, self.rank = needs, gives, cost, rank


def link_time(way, size):
    return size / (300e3 if way == "d" else 45e3)


def in_order(lists):
    clock, arrive, free, given, order = 3.0, {}, {}, set(), []
    for key, when in (("hbm", 3.5),):
        arrive[key] = when
    heads = [0] * len(lists)
    while True:
        best = None
        for number, steps in enumerate(lists):
            if heads[number] == len(steps):
                continue
            step = steps[heads[number]]
            if any(k not in given for k in step.needs) or any(k not in arrive for k in step.waits):
                continue
            ready = max([clock] + [arrive[k] for k in step.waits])
            score = (ready, step.rank, number)
            if best is None or score < best[0]:
                best = (score, number, step)
        if best is None:
            break
        (ready, _, _), number, step = best
        heads[number] += 1
        clock = ready + step.cost
        for way, size, key in step.sends:
            done = max(free.get(way, 0.0), clock) + link_time(way, size)
            free[way] = done
            arrive[key] = max(arrive.get(key, 0.0), done + (1.0 if way == "d" else 2.2))
        if step.gives is not None:
            given.add(step.gives)
        order.append((clock, step))
    assert all(h == len(s) for h, s in zip(heads, lists))
    return order


class Sems:
    def __init__(self, ref):
        self.ref, self.at = ref, {}

    def __getitem__(self, key):
        if key not in self.at:
            self.at[key] = len(self.at)
        return self.ref.at[self.at[key]]


NSEM_RECV = 192
NSEM_SEND = 24


def layer_kernel(
    tokens, w_gate, w_up, w_down, w_query, w_key, w_value, w_outgate, w_mix, cos_t, sin_t,
    gain_one, gain_mix, gain_two, s_gate, s_up, s_down, s_query, s_key, s_value, s_outgate,
    ret_gain, decay, s_mix,
    out,
    W_gu, W_dn, W_qk, W_mx,
    F_gu, F_dn, F_qk, F_mx,
    COS, SIN, DEC, GB, XG, NX, HID, QB, MX, OB, PB, RD, SB, R1, FIN, OUT,
    hbm_sem, recv_sem, send_sem,
):
    fs, tp = lax.axis_index("fs"), lax.axis_index("tp")
    z, y = fs // 4, fs % 4
    x, c = tp // 2, tp % 2

    def around(v, k):
        return (v + k) % 4

    def fs_of(zz, yy):
        return zz * 4 + yy

    def tp_of(k, core):
        return around(x, k) * 2 + core

    where = {
        "x+": (fs, tp_of(1, c)), "x-": (fs, tp_of(3, c)), "d": (fs, x * 2 + (1 - c)),
        "y+": (fs_of(z, around(y, 1)), tp), "y-": (fs_of(z, around(y, 3)), tp),
        "z+": (fs_of(around(z, 1), y), tp), "z-": (fs_of(around(z, 3), y), tp),
    }
    W = {"gu": W_gu, "dn": W_dn, "qk": W_qk, "mx": W_mx}
    recv, sent = Sems(recv_sem), Sems(send_sem)

    def copy(src, dst, send_key, recv_key, way):
        return pltpu.make_async_remote_copy(
            src_ref=src, dst_ref=dst, send_sem=sent[send_key], recv_sem=recv[recv_key],
            device_id=where[way], device_id_type=MESH,
        )

    def send(ref, send_key, recv_key, way, dst=None):
        copy(ref, ref if dst is None else dst, send_key, recv_key, way).start()

    def got(ref, send_key, recv_key):
        copy(ref, ref, send_key, recv_key, "d").wait_recv()

    def left(ref, send_key, recv_key):
        copy(ref, ref, send_key, recv_key, "d").wait_send()

    loads = {}

    def load(key, src, dst):
        loads[key] = pltpu.make_async_copy(src, dst, hbm_sem.at[len(loads)])
        loads[key].start()

    load("g", w_gate, F_gu.at[0])
    load("u", w_up, F_gu.at[1])
    for k in range(CHUNKS):
        load(("t", k), tokens.at[pl.ds(k * ROWS, ROWS), :], XG.at[k, tp])
    load("d", w_down, F_dn)
    for n, w in enumerate((w_query, w_key, w_value, w_outgate)):
        load(("q", n), w, F_qk.at[n])
    load("m", w_mix, F_mx)
    load("cos", cos_t, COS)
    load("sin", sin_t, SIN)

    barrier = pltpu.get_barrier_semaphore()
    for way in ("x+", "x-", "d", "y+", "y-", "z+", "z-"):
        pl.semaphore_signal(barrier, inc=1, device_id=where[way], device_id_type=MESH)

    lists = []

    def wpart(g, f, half, quarter=None):
        n = PIECE_ROWS[g] // 2
        lo = n * half
        if quarter is not None:
            n //= 2
            lo += n * quarter
        if g in ("gu", "qk"):
            return W[g].at[pl.ds(pl.multiple_of(f * 128 + lo, 32), n), :]
        return W[g].at[pl.ds(lo, n), pl.ds(pl.multiple_of(f * 128, 128), 128)]

    def wspan(g, pieces):
        if g in ("gu", "qk"):
            return W[g].at[pl.ds(0, 128 * pieces), :]
        return W[g].at[:, pl.ds(0, 128 * pieces)]

    def cast_gu():
        loads["g"].wait()
        loads["u"].wait()
        rows = pl.ds(pl.multiple_of(fs * 128, 128), 128)
        for j in range(3):
            W_gu[rows, 256 * j : 256 * j + 128] = F_gu[0, :, 128 * j : 128 * j + 128].astype(BF16)
            W_gu[rows, 256 * j + 128 : 256 * j + 256] = F_gu[1, :, 128 * j : 128 * j + 128].astype(BF16)

    def cast_dn():
        loads["d"].wait()
        W_dn[:, pl.ds(pl.multiple_of(fs * 128, 128), 128)] = F_dn[...].astype(BF16)

    def cast_qk():
        rows = pl.ds(pl.multiple_of(fs * 128, 128), 128)
        for n in range(4):
            loads[("q", n)].wait()
            W_qk[rows, 256 * n : 256 * n + 256] = F_qk[n].astype(BF16)

    def cast_mx():
        loads["m"].wait()
        W_mx[:, pl.ds(pl.multiple_of(fs * 128, 128), 128)] = F_mx[...].astype(BF16)

    casts = {"gu": cast_gu, "dn": cast_dn, "qk": cast_qk, "mx": cast_mx}
    cast_steps = []
    for n, g in enumerate(GROUPS):
        cast_steps.append(Step(casts[g], waits=("hbm",), gives=("cast", g), cost=0.3, rank=-5 if n == 0 else 1.5))
    lists.append(cast_steps)

    def weight_lists(order, g):
        rank = 0.2 + 0.1 * order
        for half in (0, 1):
            a, b = ("y", "z") if half == 0 else ("z", "y")

            def at(i, j, a=a):
                return fs_of(around(z, j), around(y, i)) if a == "y" else fs_of(around(z, i), around(y, j))

            full = PIECE_BYTES[g] // 2
            key = lambda *k, half=half: ("w", g, half) + k
            skey = ("w", g)

            def both(i, half=half, at=at, a=a, b=b, key=key, full=full):
                def run():
                    for way in (b + "+", b + "-"):
                        send(wpart(g, at(i, 0), half), skey, key("s", i, way[1]), way)
                return run, [(way, full, key("s", i, way[1])) for way in (b + "+", b + "-")]

            def own(half=half, at=at, a=a, b=b, key=key, full=full):
                more, extra = both(0)
                def run():
                    for way in (a + "+", a + "-"):
                        send(wpart(g, at(0, 0), half), skey, key("f", way[1]), way)
                    more()
                return run, [(way, full, key("f", way[1])) for way in (a + "+", a + "-")] + extra

            def first(side, half=half, at=at, a=a, b=b, key=key, full=full):
                i, back, q = (3, "+", 0) if side == "+" else (1, "-", 1)
                more, extra = both(i)
                def run():
                    got(wpart(g, at(i, 0), half), skey, key("f", side))
                    send(wpart(g, at(i, 0), half, q), skey, key("f2"), a + back)
                    more()
                return run, [(a + back, full // 2, key("f2"))] + extra

            def far(half=half, at=at, a=a, b=b, key=key):
                more, extra = both(2)
                def run():
                    got(wpart(g, at(2, 0), half), skey, key("f2"))
                    more()
                return run, extra

            def second(i, side, half=half, at=at, a=a, b=b, key=key, full=full):
                j, back, q = (3, "+", 0) if side == "+" else (1, "-", 1)
                def run():
                    got(wpart(g, at(i, j), half), skey, key("s", i, side))
                    send(wpart(g, at(i, j), half, q), skey, ("w", g, "end"), b + back)
                return run, [(b + back, full // 2, ("w", g, "end"))]

            run, sends = own()
            needs = [("cast", g)]
            if order:
                needs += [("far", GROUPS[order - 1], 0), ("far", GROUPS[order - 1], 1)]
            steps = [Step(run, sends=sends, needs=needs, gives=("own", g, half), rank=rank, cost=0.1)]
            for side in ("+", "-"):
                run, sends = first(side)
                steps.append(Step(run, waits=(key("f", side),), sends=sends, rank=rank))
            run, sends = far()
            steps.append(Step(run, waits=(key("f2"),), sends=sends, rank=rank, gives=("far", g, half)))
            lists.append(steps)
            steps = []
            for i in (0, 3, 1, 2):
                for side in ("+", "-"):
                    run, sends = second(i, side)
                    steps.append(Step(run, waits=(key("s", i, side),), sends=sends, rank=rank))
            steps[-1].gives = ("last", g, half)
            lists.append(steps)

        def end():
            got(wspan(g, 4), ("w", g), ("w", g, "end"))
        lists.append([Step(end, waits=(("w", g, "end"),), needs=(("last", g, 0), ("last", g, 1)), gives=("W", g), rank=rank)])

    for order, g in enumerate(GROUPS):
        weight_lists(order, g)

    def tables():
        loads["cos"].wait()
        loads["sin"].wait()
        n = lax.broadcasted_iota(jnp.int32, (LEN, LEN), 0)
        m = lax.broadcasted_iota(jnp.int32, (LEN, LEN), 1)
        distance = jnp.maximum(n - m, 0).astype(F32)
        DEC[...] = jnp.where(n >= m, jnp.exp(-decay[...] * distance), 0.0) * (LEN ** -0.5)

    lists.append([Step(tables, waits=("hbm",), gives="tables", rank=3.0, cost=0.3)])

    def chunk_list(k):
        steps = []
        base = 0.0 + 0.01 * k

        for s in range(3):
            n = s * CHUNKS + k
            xg = XG.at[n]
            akey, rkey = ("a", n), ("r", n)

            def slot(t, n=n):
                return XG.at[n, t]

            def half_of(t, h, n=n):
                return XG.at[n, t, pl.ds(128 * h, 128), :]

            gains = s == 0 and k == 0

            def a0(s=s, akey=akey, slot=slot, gains=gains):
                if s == 0:
                    loads[("t", k)].wait()
                for way, r in (("x+", "L"), ("x-", "R"), ("d", "D")):
                    send(slot(tp), akey, akey + (r,), way)
                if gains:
                    for i, gain in enumerate((gain_one, gain_mix, gain_two)):
                        GB[tp, i : i + 1, :] = gain[...]
                    for way, r in (("x+", "L"), ("x-", "R"), ("d", "D")):
                        send(GB.at[tp], ("g",), ("g", r), way)

            def a1(akey=akey, slot=slot, half_of=half_of, gains=gains):
                t = tp_of(3, c)
                got(slot(t), akey, akey + ("L",))
                send(half_of(t, 0), akey, akey + ("F",), "x+")
                send(slot(t), akey, akey + ("D",), "d")
                if gains:
                    got(GB.at[t], ("g",), ("g", "L"))
                    send(GB.at[t], ("g",), ("g", "F"), "x+")
                    send(GB.at[t], ("g",), ("g", "D"), "d")

            def a2(akey=akey, slot=slot, half_of=half_of, gains=gains):
                t = tp_of(1, c)
                got(slot(t), akey, akey + ("R",))
                send(half_of(t, 1), akey, akey + ("F",), "x-")
                send(slot(t), akey, akey + ("D",), "d")
                if gains:
                    got(GB.at[t], ("g",), ("g", "R"))
                    send(GB.at[t], ("g",), ("g", "D"), "d")

            def a3(akey=akey, slot=slot, gains=gains):
                t = tp_of(2, c)
                got(slot(t), akey, akey + ("F",))
                send(slot(t), akey, akey + ("D",), "d")
                if gains:
                    got(GB.at[t], ("g",), ("g", "F"))
                    send(GB.at[t], ("g",), ("g", "D"), "d")

            def normed(n=n, s=s, akey=akey, gains=gains):
                got(XG.at[n, pl.ds(0, 4)], akey, akey + ("D",))
                if gains:
                    got(GB.at[pl.ds(0, 4)], ("g",), ("g", "D"))

                def rows_of(i, carry):
                    r = pl.ds(pl.multiple_of(i * 16, 16), 16)
                    hs = [XG[n, t, r, :].astype(F32) for t in range(8)]
                    squares = hs[0] * hs[0]
                    for h in hs[1:]:
                        squares += h * h
                    scale = lax.rsqrt(jnp.sum(squares, axis=1, keepdims=True) / D + EPS)
                    for t in range(8):
                        NX[r, 256 * t : 256 * t + 256] = (hs[t] * scale * GB[t, s : s + 1, :]).astype(BF16)
                    return carry

                lax.fori_loop(0, ROWS // 16, rows_of, 0)

            def gate_up(normed=normed):
                normed()

                def cols_of(j, carry):
                    both = jnp.dot(
                        NX[...], W_gu[:, pl.ds(pl.multiple_of(j * 256, 256), 256)], preferred_element_type=F32
                    )
                    lane = pl.ds(pl.multiple_of(j * 128, 128), 128)
                    gate, up = both[:, :128] * s_gate[:, lane], both[:, 128:] * s_up[:, lane]
                    HID[k, :, lane] = (gate / (1.0 + jnp.exp(-gate)) * up).astype(BF16)
                    return carry

                lax.fori_loop(0, 3, cols_of, 0)

            def query_key(normed=normed):
                normed()
                for j, scale in enumerate((s_query, s_key, s_value, s_outgate)):
                    pre = jnp.dot(NX[...], W_qk[:, 256 * j : 256 * j + 256], preferred_element_type=F32)
                    QB[j] = (pre * scale[...]).astype(BF16)

            def turned(j):
                v = QB[j].astype(F32)
                even = lax.broadcasted_iota(jnp.int32, (LEN, 256), 1) % 2 == 0
                swapped = jnp.where(even, -pltpu.roll(v, 255, 1), pltpu.roll(v, 1, 1))
                return (v * COS[...] + swapped * SIN[...]).astype(BF16)

            def retained():
                scores = lax.dot_general(
                    turned(0), turned(1), (((1,), (1,)), ((), ())), preferred_element_type=F32
                )
                kept = jnp.dot((scores * DEC[...]).astype(BF16), QB[2], preferred_element_type=F32)
                kept = kept * lax.rsqrt(jnp.mean(kept * kept, axis=1, keepdims=True) + HEAD_EPS)
                gate = QB[3].astype(F32)
                MX[...] = (kept * ret_gain[...] * (gate / (1.0 + jnp.exp(-gate)))).astype(BF16)

            def product(i, core, s=s):
                cols = pl.ds(pl.multiple_of((around(x, i) * 2 + core) * 256, 256), 256)
                if s == 1:
                    return jnp.dot(MX[...], W_mx[:, cols], preferred_element_type=F32)
                return jnp.dot(HID[k], W_dn[:, cols], preferred_element_type=F32)

            def theirs(n=n, rkey=rkey, product=product):
                def block_of(i, carry):
                    PB[n, i] = product(i, 1 - c).astype(BF16)
                    return carry

                lax.fori_loop(0, 4, block_of, 0)
                for i, r in ((2, "2"), (1, "13"), (3, "13"), (0, "0")):
                    send(PB.at[n, i], rkey, rkey + (r,), "d", RD.at[n, i])

            def mine(product=product):
                def block_of(i, carry):
                    OB[k, i] = product(i, c)
                    return carry

                lax.fori_loop(0, 4, block_of, 0)

            def r0(n=n, rkey=rkey):
                got(RD.at[n, 2], rkey, rkey + ("2",))
                SB[n, 0] = (OB[k, 2] + RD[n, 2].astype(F32)).astype(BF16)
                send(SB.at[n, 0, pl.ds(0, 128)], rkey, rkey + ("L",), "x+", R1.at[n, 0])
                send(SB.at[n, 0, pl.ds(128, 128)], rkey, rkey + ("R",), "x-", R1.at[n, 1])

            def r1(n=n, rkey=rkey):
                got(RD.at[n, pl.ds(0, 2)], rkey, rkey + ("13",))
                upper = OB[k, 1, 128:256] + RD[n, 1, 128:256].astype(F32)
                SB[n, 1, 128:256] = upper.astype(BF16)
                send(SB.at[n, 1, pl.ds(128, 128)], rkey, rkey + ("E",), "x+", FIN.at[n, 0, pl.ds(128, 128)])
                lower = OB[k, 3, 0:128] + RD[n, 3, 0:128].astype(F32)
                SB[n, 2, 0:128] = lower.astype(BF16)
                send(SB.at[n, 2, pl.ds(0, 128)], rkey, rkey + ("E",), "x-", FIN.at[n, 1, pl.ds(0, 128)])

            def r2(n=n, rkey=rkey):
                got(R1.at[n, 0], rkey, rkey + ("L",))
                SB[n, 1, 0:128] = (
                    OB[k, 1, 0:128] + RD[n, 1, 0:128].astype(F32) + R1[n, 0].astype(F32)
                ).astype(BF16)
                send(SB.at[n, 1, pl.ds(0, 128)], rkey, rkey + ("E",), "x+", FIN.at[n, 0, pl.ds(0, 128)])

            def r3(n=n, rkey=rkey):
                got(R1.at[n, 1], rkey, rkey + ("R",))
                SB[n, 2, 128:256] = (
                    OB[k, 3, 128:256] + RD[n, 3, 128:256].astype(F32) + R1[n, 1].astype(F32)
                ).astype(BF16)
                send(SB.at[n, 2, pl.ds(128, 128)], rkey, rkey + ("E",), "x-", FIN.at[n, 1, pl.ds(128, 128)])

            def r4(n=n, s=s, rkey=rkey):
                got(RD.at[n, 0], rkey, rkey + ("0",))
                got(FIN.at[n], rkey, rkey + ("E",))
                total = OB[k, 0] + RD[n, 0].astype(F32) + FIN[n, 0].astype(F32) + FIN[n, 1].astype(F32)
                if s == 1:
                    total = total * s_mix[...]
                else:
                    total = 0.5 * total * s_down[...]
                after = (XG[n, tp].astype(F32) + total).astype(BF16)
                if s < 2:
                    XG[n + CHUNKS, tp] = after
                else:
                    OUT[k] = after
                    pltpu.make_async_copy(OUT.at[k], out.at[pl.ds(k * ROWS, ROWS), :], hbm_sem.at[20 + k]).start()

            L, R, F, Dk = (akey + (r,) for r in "LRFD")
            extra = (("g", "L"), ("g", "R"), ("g", "F"), ("g", "D"))
            sends = [("x+", BLOCK, L), ("x-", BLOCK, R), ("d", BLOCK, Dk)]
            waits = ("hbm",) if s == 0 else ()
            gsize = 8192
            add = lambda *pairs: [(w, gsize, q) for w, q in pairs] if gains else []
            more = lambda q: (q,) if gains else ()
            a0_step = Step(a0, waits=waits, sends=sends + add(("x+", extra[0]), ("x-", extra[1]), ("d", extra[3])),
                           rank=base + (0.0 if s else -1 + 0.1 * k), cost=0.1)
            steps.append(a0_step)
            steps.append(Step(a1, waits=(L,) + more(extra[0]),
                              sends=[("x+", BLOCK // 2, F), ("d", BLOCK, Dk)] + add(("x+", extra[2]), ("d", extra[3])), rank=base))
            steps.append(Step(a2, waits=(R,) + more(extra[1]),
                              sends=[("x-", BLOCK // 2, F), ("d", BLOCK, Dk)] + add(("d", extra[3])), rank=base))
            steps.append(Step(a3, waits=(F,) + more(extra[2]), sends=[("d", BLOCK, Dk)] + add(("d", extra[3])), rank=base))
            if s == 1:
                steps.append(Step(query_key, waits=(Dk,), needs=(("W", "qk"),), rank=2 + base, cost=2.0))
                steps.append(Step(retained, needs=("tables",), rank=2 + base, cost=0.7))
                end = ("W", "mx")
            else:
                needs = (("W", "gu"),) if gains else (("W", "gu"), "gains")
                steps.append(Step(gate_up, waits=(Dk,) + more(extra[3]), needs=needs, rank=2 + base, cost=1.8,
                                  gives="gains" if gains else None))
                end = ("W", "dn")
            r = lambda q: rkey + (q,)
            steps.append(Step(theirs, needs=(end,), rank=2 + base, cost=0.5,
                              sends=[("d", BLOCK, r("2")), ("d", BLOCK, r("13")), ("d", BLOCK, r("13")), ("d", BLOCK, r("0"))]))
            steps.append(Step(mine, rank=2 + base, cost=0.5))
            steps.append(Step(r0, waits=(r("2"),), rank=base, sends=[("x+", BLOCK // 2, r("L")), ("x-", BLOCK // 2, r("R"))], cost=0.15))
            steps.append(Step(r1, waits=(r("13"),), rank=base, sends=[("x+", BLOCK // 2, r("E")), ("x-", BLOCK // 2, r("E"))], cost=0.15))
            steps.append(Step(r2, waits=(r("L"),), rank=base, sends=[("x+", BLOCK // 2, r("E"))]))
            steps.append(Step(r3, waits=(r("R"),), rank=base, sends=[("x-", BLOCK // 2, r("E"))]))
            steps.append(Step(r4, waits=(r("E"), r("0")), rank=base, cost=0.2))
        return steps

    for k in range(CHUNKS):
        lists.append(chunk_list(k))

    order = in_order(lists)
    pl.semaphore_wait(barrier, 7)
    for _, step in order:
        step.run()

    for g in GROUPS:
        left(wspan(g, 15), ("w", g), ("w", g, "end"))
    left(GB.at[pl.ds(0, 7)], ("g",), ("g", "D"))
    for n in range(3 * CHUNKS):
        left(XG.at[n, pl.ds(0, 7)], ("a", n), ("a", n, "D"))
        left(XG.at[n, pl.ds(0, 7)], ("r", n), ("r", n, "0"))
    for k in range(CHUNKS):
        pltpu.make_async_copy(OUT.at[k], out.at[pl.ds(k * ROWS, ROWS), :], hbm_sem.at[20 + k]).wait()
    assert len(recv.at) <= NSEM_RECV and len(sent.at) <= NSEM_SEND


def per_device(
    tokens, gain_one, w_gate, w_up, w_down, scale_gate, scale_up, scale_down, gain_mix,
    w_query, w_key, w_value, w_outgate, scale_query, scale_key, scale_value, scale_outgate,
    ret_gain, decay_rate, w_mix, scale_mix, gain_two,
):
    freq = (1.0 / 10000.0 ** np.linspace(0.0, 1.0, 128)).astype(np.float32)
    angles = (np.arange(LEN, dtype=np.float32)[:, None] * np.repeat(freq, 2)[None, :]).astype(np.float64)
    cos_t = jnp.asarray(np.cos(angles), F32)
    sin_t = jnp.asarray(np.sin(angles), F32)
    row = lambda v: v.reshape(1, -1)
    small = [row(v) for v in (
        gain_one, gain_mix, gain_two, scale_gate, scale_up, scale_down, scale_query, scale_key, scale_value,
        scale_outgate, ret_gain, decay_rate, scale_mix,
    )]
    anywhere = pl.BlockSpec(memory_space=pl.ANY)
    vmem = pl.BlockSpec(memory_space=pltpu.VMEM)
    V = pltpu.VMEM
    nine = 3 * CHUNKS
    return pl.pallas_call(
        layer_kernel,
        out_shape=jax.ShapeDtypeStruct((CHUNKS * ROWS, 256), BF16),
        in_specs=[anywhere] * 11 + [vmem] * len(small),
        out_specs=anywhere,
        scratch_shapes=[
            V((2048, 768), BF16), V((384, 2048), BF16), V((2048, 1024), BF16), V((256, 2048), BF16),
            V((2, 128, 384), F32), V((384, 128), F32), V((4, 128, 256), F32), V((256, 128), F32),
            V((LEN, 256), F32), V((LEN, 256), F32), V((LEN, LEN), F32), V((8, 8, 256), F32),
            V((nine, 8, ROWS, 256), BF16), V((ROWS, D), BF16), V((CHUNKS, ROWS, 384), BF16),
            V((4, ROWS, 256), BF16), V((ROWS, 256), BF16), V((CHUNKS, 4, ROWS, 256), F32),
            V((nine, 4, ROWS, 256), BF16), V((nine, 4, ROWS, 256), BF16), V((nine, 3, ROWS, 256), BF16),
            V((nine, 2, 128, 256), BF16), V((nine, 2, ROWS, 256), BF16), V((CHUNKS, ROWS, 256), BF16),
            pltpu.SemaphoreType.DMA((24,)), pltpu.SemaphoreType.DMA((NSEM_RECV,)), pltpu.SemaphoreType.DMA((NSEM_SEND,)),
        ],
        compiler_params=pltpu.CompilerParams(
            collective_id=0, has_side_effects=True, vmem_limit_bytes=60 * 1024 * 1024
        ),
        name="layer",
    )(tokens, w_gate, w_up, w_down, w_query, w_key, w_value, w_outgate, w_mix, cos_t, sin_t, *small)


def solution(mesh):
    return jax.shard_map(
        per_device,
        mesh=mesh,
        in_specs=(
            P("fs", "tp"), P("tp"), P("fs", "tp"), P("fs", "tp"), P("tp", "fs"), P("tp"), P("tp"), P("tp"), P("tp"),
            P("fs", "tp"), P("fs", "tp"), P("fs", "tp"), P("fs", "tp"), P("tp"), P("tp"), P("tp"), P("tp"), P("tp"),
            P("tp"), P("tp", "fs"), P("tp"), P("tp"),
        ),
        out_specs=P("fs", "tp"),
        check_vma=False,
    )
```

time: 381 us -> 144 us (0.38)
  waiting for transfers between devices: 150 us -> 0 us
  Pallas kernels: 0 us -> 139 us
  blocking collectives: 110 us -> 0 us
  matrix products: 42.7 us -> 0 us
  other arithmetic: 25.7 us -> 0 us
  starting transfers between devices: 17.2 us -> 0 us
  local copies, waits for them, and re-layouts: 20.2 us -> 3.72 us
  between operations: 14.5 us -> 0.67 us
    pallas_call x0 -> x1, Pallas kernels: none -> 139 us  [per_device(): pl.pallas_call(layer_kernel, out_shape=jax.ShapeDtypeStruct((CHUNKS * ROW...]
    all_gather x5 -> x0, waiting for transfers between devices: 111 us -> none  [the longest x3 60 us: normed_rows(): return lax.all_gather(scaled.astype(jnp.bfloat16), 'tp', axis=1, tiled=True)]
    all_to_all x5 -> x0, blocking collectives: 110 us -> none  [the longest x2 84.4 us: sent_and_summed(): lax.all_to_all(in_blocks(shard, dim, length), axis, 0, 0, tiled=True)]
    dot_general x15 -> x0, matrix products: 42.7 us -> none  [the longest x2 13.3 us: ffn_gathered(): jnp.dot(hidden, gathered_copies(down_low, 'fs', 1), preferred_element_typ...]
    all_to_all x3 -> x0, waiting for transfers between devices: 38.3 us -> none  [the longest x1 38.3 us: sent_and_summed(): lax.all_to_all(in_blocks(shard, dim, length), axis, 0, 0, tiled=True)]
    all_to_all x3 -> x0, starting transfers between devices: 16.8 us -> none  [the longest x2 12.4 us: from_everyone(): return lax.all_to_all(copies, axis, split_axis=0, concat_axis=0, tiled=True)]
    cos x1 -> x0, other arithmetic: 8.54 us -> none  [retain(): cosines = jnp.cos(angles)[None, :, None, :]]
    convert_element_type x12 -> x0, other arithmetic: 8.37 us -> none  [the longest x3 3.75 us: normed_rows(): return lax.all_gather(scaled.astype(jnp.bfloat16), 'tp', axis=1, tiled=True)]
  transfers between devices with their start and end apart: 8 -> 0, of which waited for: 5 -> 0; matrix products, arithmetic and copies ran while one was open for 17% -> 0% of each run, Pallas kernels for 0% -> 0%
where the time goes in v1:
time: 144 us; the launch traced here: 143 us
  Pallas kernels  139 us (97%)
  local copies, waits for them, and re-layouts  3.72 us (3%)
    pallas_call x1, Pallas kernels, per_device(): pl.pallas_call(layer_kernel, out_shape=jax.ShapeDtypeStruct((CHUNKS * ROW...  139 us

profile of v1, /device:TPU:0, one launch (start us, length us, event | category | flops | bytes accessed | tf_op | source)
XLA Modules:
  0.0 143.4 jit_solution(14281365372315906627)
XLA Ops:
  0.7 0.0 copy-start
  0.7 0.7 copy-done
  1.3 0.0 copy-start.1
  1.3 0.6 reshape.42.s_gate
  1.9 0.1 copy-done.1
  2.0 0.6 reshape.43.s_up
  2.6 139.0 %layer.1 = bf16[768,256]{1,0:T(8,128)(2,1)} custom-call(bf16[768,256]{1,0:T(8,128)(2,1)} %tokens.1, f32[128,384]{1,0:T(8,128)} %w_gate.1, f32[128,384]{1,0:T(8,128)} %w_up.1, f32[384,128]{1,0:T(8,128)} %w_down.1, f32[128,256]{1,0:T(8,128)} %w_query.1, f32[128,256]{1,0:T(8,128)} %w_key.1, f32[128,256]{1,0:T(8,128)} %w_value.1, f32[128,256]{1,0:T(8,128)} %w_outgate.1, ...), custom_call_target="tpu_custom_call" | custom-call | tf_op jit(solution)/shard_map/layer/pallas_call | solution.py:527
  141.6 1.8 %copy.27 = bf16[768,256]{1,0:T(8,128)(2,1)} copy(bf16[768,256]{1,0:T(8,128)(2,1)} %layer.1) | data formatting | bytes 786432
Async XLA Ops:
  0.7 0.7 copy-start
  1.3 0.7 copy-start.1

commit v2 on v1

--- a/solution.py
+++ b/solution.py
@@ -14,55 +14,92 @@
 
 D = 2048
 LEN = 256
-ROWS = 256
-CHUNKS = 3
+ROWS = 128
+HALF = ROWS // 2
+CHUNKS = 6
 EPS = 1e-06
 HEAD_EPS = 0.1
 GROUPS = ("gu", "dn", "qk", "mx")
 PIECE_ROWS = {"gu": 128, "dn": 384, "qk": 128, "mx": 256}
 PIECE_BYTES = {"gu": 196608, "dn": 98304, "qk": 262144, "mx": 65536}
-BLOCK = 131072
+BLOCK = ROWS * 512
 
 
 class Step:
-    def __init__(self, run, waits=(), sends=(), needs=(), gives=None, cost=0.1, rank=1.0):
+    def __init__(self, run, waits=(), sends=(), needs=(), gives=None, cost=0.02, rank=1.0):
         self.run, self.waits, self.sends = run, waits, sends
         self.needs, self.gives, self.cost, self.rank = needs, gives, cost, rank
 
 
+START = 1.5
+MARGIN = 0.3
+LATENCY = 2.6
+WAYS = ("x+", "x-", "d", "y+", "y-", "z+", "z-")
+GROUP_GAP = 2.5
+STAGE_GAP = 10.0
+COST = {"norm": 0.37, "gu": 0.73, "qk": 0.83, "ret": 0.4, "dn": 0.32, "mx": 0.25}
+GATE = (None, None, None)
+
+
 def link_time(way, size):
-    return size / (300e3 if way == "d" else 45e3)
+    return size / (300e3 if way == "d" else 45.7e3)
 
 
 def in_order(lists):
-    clock, arrive, free, given, order = 3.0, {}, {}, set(), []
-    for key, when in (("hbm", 3.5),):
-        arrive[key] = when
+    clock, free, given, order = 0.0, {}, set(), []
+    arrive = {"hbm": 0.5}
+    for way in WAYS:
+        free[way] = START
+    pending = {way: [] for way in WAYS}
     heads = [0] * len(lists)
+    count = 0
+
+    def issue(way, entry):
+        _, _, size, key, step, which = entry
+        done = max(free[way], clock) + link_time(way, size)
+        free[way] = done
+        arrive[key] = max(arrive.get(key, 0.0), done + (0.9 if way == "d" else LATENCY))
+        missing[key] -= 1
+        order.append((clock, step, which))
+
+    missing = {"hbm": 0}
+    for steps in lists:
+        for step in steps:
+            for _, _, key, _ in step.sends:
+                missing[key] = missing.get(key, 0) + 1
+
     while True:
         best = None
         for number, steps in enumerate(lists):
             if heads[number] == len(steps):
                 continue
             step = steps[heads[number]]
-            if any(k not in given for k in step.needs) or any(k not in arrive for k in step.waits):
+            if any(k not in given for k in step.needs) or any(missing[k] for k in step.waits):
                 continue
             ready = max([clock] + [arrive[k] for k in step.waits])
             score = (ready, step.rank, number)
             if best is None or score < best[0]:
                 best = (score, number, step)
+        horizon = 1e9 if best is None else best[0][0] + best[2].cost + MARGIN
+        issued = False
+        for way in WAYS:
+            if pending[way] and (way == "d" or free[way] < horizon):
+                pending[way].sort(key=lambda e: e[:2])
+                issue(way, pending[way].pop(0))
+                issued = True
+        if issued:
+            continue
         if best is None:
             break
         (ready, _, _), number, step = best
         heads[number] += 1
         clock = ready + step.cost
-        for way, size, key in step.sends:
-            done = max(free.get(way, 0.0), clock) + link_time(way, size)
-            free[way] = done
-            arrive[key] = max(arrive.get(key, 0.0), done + (1.0 if way == "d" else 2.2))
         if step.gives is not None:
             given.add(step.gives)
-        order.append((clock, step))
+        order.append((clock, step, None))
+        for which, (way, size, key, urgency) in enumerate(step.sends):
+            pending[way].append((urgency, count, size, key, step, which))
+            count += 1
     assert all(h == len(s) for h, s in zip(heads, lists))
     return order
 
@@ -77,8 +114,8 @@
         return self.ref.at[self.at[key]]
 
 
-NSEM_RECV = 192
-NSEM_SEND = 24
+NSEM_RECV = 288
+NSEM_SEND = 48
 
 
 def layer_kernel(
@@ -88,7 +125,7 @@
     out,
     W_gu, W_dn, W_qk, W_mx,
     F_gu, F_dn, F_qk, F_mx,
-    COS, SIN, DEC, GB, XG, NX, HID, QB, MX, OB, PB, RD, SB, R1, FIN, OUT,
+    COS, SIN, DEC, GB, XG, NX, HID, QB, OG, KB, VB, MX, OB, PB, RD, SB, R1, FIN, OUT,
     hbm_sem, recv_sem, send_sem,
 ):
     fs, tp = lax.axis_index("fs"), lax.axis_index("tp")
@@ -118,8 +155,10 @@
             device_id=where[way], device_id_type=MESH,
         )
 
+    held = []
+
     def send(ref, send_key, recv_key, way, dst=None):
-        copy(ref, ref if dst is None else dst, send_key, recv_key, way).start()
+        held.append((way, lambda: copy(ref, ref if dst is None else dst, send_key, recv_key, way).start()))
 
     def got(ref, send_key, recv_key):
         copy(ref, ref, send_key, recv_key, "d").wait_recv()
@@ -145,7 +184,7 @@
     load("sin", sin_t, SIN)
 
     barrier = pltpu.get_barrier_semaphore()
-    for way in ("x+", "x-", "d", "y+", "y-", "z+", "z-"):
+    for way in WAYS:
         pl.semaphore_signal(barrier, inc=1, device_id=where[way], device_id_type=MESH)
 
     lists = []
@@ -190,11 +229,12 @@
     casts = {"gu": cast_gu, "dn": cast_dn, "qk": cast_qk, "mx": cast_mx}
     cast_steps = []
     for n, g in enumerate(GROUPS):
-        cast_steps.append(Step(casts[g], waits=("hbm",), gives=("cast", g), cost=0.3, rank=-5 if n == 0 else 1.5))
+        cast_steps.append(Step(casts[g], waits=("hbm",), gives=("cast", g), cost=0.05, rank=-5 if n == 0 else 1.5))
     lists.append(cast_steps)
 
     def weight_lists(order, g):
         rank = 0.2 + 0.1 * order
+        base = GROUP_GAP * order
         for half in (0, 1):
             a, b = ("y", "z") if half == 0 else ("z", "y")
 
@@ -209,7 +249,7 @@
                 def run():
                     for way in (b + "+", b + "-"):
                         send(wpart(g, at(i, 0), half), skey, key("s", i, way[1]), way)
-                return run, [(way, full, key("s", i, way[1])) for way in (b + "+", b + "-")]
+                return run, [(way, full, key("s", i, way[1]), base + (2 if i else 1.5)) for way in (b + "+", b + "-")]
 
             def own(half=half, at=at, a=a, b=b, key=key, full=full):
                 more, extra = both(0)
@@ -217,7 +257,7 @@
                     for way in (a + "+", a + "-"):
                         send(wpart(g, at(0, 0), half), skey, key("f", way[1]), way)
                     more()
-                return run, [(way, full, key("f", way[1])) for way in (a + "+", a + "-")] + extra
+                return run, [(way, full, key("f", way[1]), base) for way in (a + "+", a + "-")] + extra
 
             def first(side, half=half, at=at, a=a, b=b, key=key, full=full):
                 i, back, q = (3, "+", 0) if side == "+" else (1, "-", 1)
@@ -226,7 +266,7 @@
                     got(wpart(g, at(i, 0), half), skey, key("f", side))
                     send(wpart(g, at(i, 0), half, q), skey, key("f2"), a + back)
                     more()
-                return run, [(a + back, full // 2, key("f2"))] + extra
+                return run, [(a + back, full // 2, key("f2"), base + 1)] + extra
 
             def far(half=half, at=at, a=a, b=b, key=key):
                 more, extra = both(2)
@@ -240,16 +280,17 @@
                 def run():
                     got(wpart(g, at(i, j), half), skey, key("s", i, side))
                     send(wpart(g, at(i, j), half, q), skey, ("w", g, "end"), b + back)
-                return run, [(b + back, full // 2, ("w", g, "end"))]
+                return run, [(b + back, full // 2, ("w", g, "end"), base + 3)]
 
             run, sends = own()
             needs = [("cast", g)]
-            if order:
-                needs += [("far", GROUPS[order - 1], 0), ("far", GROUPS[order - 1], 1)]
-            steps = [Step(run, sends=sends, needs=needs, gives=("own", g, half), rank=rank, cost=0.1)]
+            if order and GATE[order - 1]:
+                needs += [(GATE[order - 1], GROUPS[order - 1], h) for h in (0, 1)]
+            steps = [Step(run, sends=sends, needs=needs, gives=("own", g, half), rank=rank)]
             for side in ("+", "-"):
                 run, sends = first(side)
-                steps.append(Step(run, waits=(key("f", side),), sends=sends, rank=rank))
+                steps.append(Step(run, waits=(key("f", side),), sends=sends, rank=rank,
+                                  gives=("near", g, half) if side == "-" else None))
             run, sends = far()
             steps.append(Step(run, waits=(key("f2"),), sends=sends, rank=rank, gives=("far", g, half)))
             lists.append(steps)
@@ -274,13 +315,14 @@
         n = lax.broadcasted_iota(jnp.int32, (LEN, LEN), 0)
         m = lax.broadcasted_iota(jnp.int32, (LEN, LEN), 1)
         distance = jnp.maximum(n - m, 0).astype(F32)
-        DEC[...] = jnp.where(n >= m, jnp.exp(-decay[...] * distance), 0.0) * (LEN ** -0.5)
-
-    lists.append([Step(tables, waits=("hbm",), gives="tables", rank=3.0, cost=0.3)])
+        DEC[...] = jnp.where(n >= m, jnp.exp(-decay[...].reshape(1, 1) * distance), 0.0) * (LEN ** -0.5)
+
+    lists.append([Step(tables, waits=("hbm",), gives="tables", rank=3.0, cost=0.15)])
 
     def chunk_list(k):
         steps = []
         base = 0.0 + 0.01 * k
+        seq, half = k * ROWS // LEN, k % (LEN // ROWS)
 
         for s in range(3):
             n = s * CHUNKS + k
@@ -291,7 +333,7 @@
                 return XG.at[n, t]
 
             def half_of(t, h, n=n):
-                return XG.at[n, t, pl.ds(128 * h, 128), :]
+                return XG.at[n, t, pl.ds(HALF * h, HALF), :]
 
             gains = s == 0 and k == 0
 
@@ -346,96 +388,94 @@
                         squares += h * h
                     scale = lax.rsqrt(jnp.sum(squares, axis=1, keepdims=True) / D + EPS)
                     for t in range(8):
-                        NX[r, 256 * t : 256 * t + 256] = (hs[t] * scale * GB[t, s : s + 1, :]).astype(BF16)
+                        NX[k, r, 256 * t : 256 * t + 256] = (hs[t] * scale * GB[t, s : s + 1, :]).astype(BF16)
                     return carry
 
-                lax.fori_loop(0, ROWS // 16, rows_of, 0)
-
-            def gate_up(normed=normed):
-                normed()
-
-                def cols_of(j, carry):
-                    both = jnp.dot(
-                        NX[...], W_gu[:, pl.ds(pl.multiple_of(j * 256, 256), 256)], preferred_element_type=F32
-                    )
-                    lane = pl.ds(pl.multiple_of(j * 128, 128), 128)
-                    gate, up = both[:, :128] * s_gate[:, lane], both[:, 128:] * s_up[:, lane]
+                lax.fori_loop(0, ROWS // 16, rows_of, 0, unroll=4)
+
+            def gate_up():
+                for j in range(3):
+                    both = jnp.dot(NX[k], W_gu[:, 256 * j : 256 * j + 256], preferred_element_type=F32)
+                    lane = slice(128 * j, 128 * j + 128)
+                    gate = both[:, :128] * s_gate[lane].reshape(1, 128)
+                    up = both[:, 128:] * s_up[lane].reshape(1, 128)
                     HID[k, :, lane] = (gate / (1.0 + jnp.exp(-gate)) * up).astype(BF16)
-                    return carry
-
-                lax.fori_loop(0, 3, cols_of, 0)
-
-            def query_key(normed=normed):
-                normed()
-                for j, scale in enumerate((s_query, s_key, s_value, s_outgate)):
-                    pre = jnp.dot(NX[...], W_qk[:, 256 * j : 256 * j + 256], preferred_element_type=F32)
-                    QB[j] = (pre * scale[...]).astype(BF16)
-
-            def turned(j):
-                v = QB[j].astype(F32)
-                even = lax.broadcasted_iota(jnp.int32, (LEN, 256), 1) % 2 == 0
+
+            def turned(v):
+                at = slice(ROWS * half, ROWS * half + ROWS)
+                even = lax.broadcasted_iota(jnp.int32, (ROWS, 256), 1) % 2 == 0
                 swapped = jnp.where(even, -pltpu.roll(v, 255, 1), pltpu.roll(v, 1, 1))
-                return (v * COS[...] + swapped * SIN[...]).astype(BF16)
+                return (v * COS[at, :] + swapped * SIN[at, :]).astype(BF16)
+
+            def query_key():
+                at = slice(ROWS * half, ROWS * half + ROWS)
+                for j, scale in enumerate((s_key, s_value, s_query, s_outgate)):
+                    col = 256 * (1, 2, 0, 3)[j]
+                    pre = jnp.dot(NX[k], W_qk[:, col : col + 256], preferred_element_type=F32)
+                    row = (pre * scale[...]).astype(BF16)
+                    if j == 0:
+                        KB[seq, at, :] = turned(row.astype(F32))
+                    elif j == 1:
+                        VB[seq, at, :] = row
+                    elif j == 2:
+                        QB[k] = turned(row.astype(F32))
+                    else:
+                        OG[k] = row
 
             def retained():
+                seen = ROWS * half + ROWS
                 scores = lax.dot_general(
-                    turned(0), turned(1), (((1,), (1,)), ((), ())), preferred_element_type=F32
+                    QB[k], KB[seq, 0:seen, :], (((1,), (1,)), ((), ())), preferred_element_type=F32
                 )
-                kept = jnp.dot((scores * DEC[...]).astype(BF16), QB[2], preferred_element_type=F32)
+                scores = scores * DEC[ROWS * half : seen, 0:seen]
+                kept = jnp.dot(scores.astype(BF16), VB[seq, 0:seen, :], preferred_element_type=F32)
                 kept = kept * lax.rsqrt(jnp.mean(kept * kept, axis=1, keepdims=True) + HEAD_EPS)
-                gate = QB[3].astype(F32)
-                MX[...] = (kept * ret_gain[...] * (gate / (1.0 + jnp.exp(-gate)))).astype(BF16)
+                gate = OG[k].astype(F32)
+                MX[k] = (kept * ret_gain[...] * (gate / (1.0 + jnp.exp(-gate)))).astype(BF16)
 
             def product(i, core, s=s):
                 cols = pl.ds(pl.multiple_of((around(x, i) * 2 + core) * 256, 256), 256)
                 if s == 1:
-                    return jnp.dot(MX[...], W_mx[:, cols], preferred_element_type=F32)
+                    return jnp.dot(MX[k], W_mx[:, cols], preferred_element_type=F32)
                 return jnp.dot(HID[k], W_dn[:, cols], preferred_element_type=F32)
 
             def theirs(n=n, rkey=rkey, product=product):
-                def block_of(i, carry):
+                for i, r in ((2, "2"), (1, "13"), (3, "13"), (0, "0")):
                     PB[n, i] = product(i, 1 - c).astype(BF16)
-                    return carry
-
-                lax.fori_loop(0, 4, block_of, 0)
-                for i, r in ((2, "2"), (1, "13"), (3, "13"), (0, "0")):
                     send(PB.at[n, i], rkey, rkey + (r,), "d", RD.at[n, i])
 
             def mine(product=product):
-                def block_of(i, carry):
+                for i in (2, 1, 3, 0):
                     OB[k, i] = product(i, c)
-                    return carry
-
-                lax.fori_loop(0, 4, block_of, 0)
 
             def r0(n=n, rkey=rkey):
                 got(RD.at[n, 2], rkey, rkey + ("2",))
                 SB[n, 0] = (OB[k, 2] + RD[n, 2].astype(F32)).astype(BF16)
-                send(SB.at[n, 0, pl.ds(0, 128)], rkey, rkey + ("L",), "x+", R1.at[n, 0])
-                send(SB.at[n, 0, pl.ds(128, 128)], rkey, rkey + ("R",), "x-", R1.at[n, 1])
+                send(SB.at[n, 0, pl.ds(0, HALF)], rkey, rkey + ("L",), "x+", R1.at[n, 0])
+                send(SB.at[n, 0, pl.ds(HALF, HALF)], rkey, rkey + ("R",), "x-", R1.at[n, 1])
 
             def r1(n=n, rkey=rkey):
                 got(RD.at[n, pl.ds(0, 2)], rkey, rkey + ("13",))
-                upper = OB[k, 1, 128:256] + RD[n, 1, 128:256].astype(F32)
-                SB[n, 1, 128:256] = upper.astype(BF16)
-                send(SB.at[n, 1, pl.ds(128, 128)], rkey, rkey + ("E",), "x+", FIN.at[n, 0, pl.ds(128, 128)])
-                lower = OB[k, 3, 0:128] + RD[n, 3, 0:128].astype(F32)
-                SB[n, 2, 0:128] = lower.astype(BF16)
-                send(SB.at[n, 2, pl.ds(0, 128)], rkey, rkey + ("E",), "x-", FIN.at[n, 1, pl.ds(0, 128)])
+                upper = OB[k, 1, HALF:ROWS] + RD[n, 1, HALF:ROWS].astype(F32)
+                SB[n, 1, HALF:ROWS] = upper.astype(BF16)
+                send(SB.at[n, 1, pl.ds(HALF, HALF)], rkey, rkey + ("E",), "x+", FIN.at[n, 0, pl.ds(HALF, HALF)])
+                lower = OB[k, 3, 0:HALF] + RD[n, 3, 0:HALF].astype(F32)
+                SB[n, 2, 0:HALF] = lower.astype(BF16)
+                send(SB.at[n, 2, pl.ds(0, HALF)], rkey, rkey + ("E",), "x-", FIN.at[n, 1, pl.ds(0, HALF)])
 
             def r2(n=n, rkey=rkey):
                 got(R1.at[n, 0], rkey, rkey + ("L",))
-                SB[n, 1, 0:128] = (
-                    OB[k, 1, 0:128] + RD[n, 1, 0:128].astype(F32) + R1[n, 0].astype(F32)
+                SB[n, 1, 0:HALF] = (
+                    OB[k, 1, 0:HALF] + RD[n, 1, 0:HALF].astype(F32) + R1[n, 0].astype(F32)
                 ).astype(BF16)
-                send(SB.at[n, 1, pl.ds(0, 128)], rkey, rkey + ("E",), "x+", FIN.at[n, 0, pl.ds(0, 128)])
+                send(SB.at[n, 1, pl.ds(0, HALF)], rkey, rkey + ("E",), "x+", FIN.at[n, 0, pl.ds(0, HALF)])
 
             def r3(n=n, rkey=rkey):
                 got(R1.at[n, 1], rkey, rkey + ("R",))
-                SB[n, 2, 128:256] = (
-                    OB[k, 3, 128:256] + RD[n, 3, 128:256].astype(F32) + R1[n, 1].astype(F32)
+                SB[n, 2, HALF:ROWS] = (
+                    OB[k, 3, HALF:ROWS] + RD[n, 3, HALF:ROWS].astype(F32) + R1[n, 1].astype(F32)
                 ).astype(BF16)
-                send(SB.at[n, 2, pl.ds(128, 128)], rkey, rkey + ("E",), "x-", FIN.at[n, 1, pl.ds(128, 128)])
+                send(SB.at[n, 2, pl.ds(HALF, HALF)], rkey, rkey + ("E",), "x-", FIN.at[n, 1, pl.ds(HALF, HALF)])
 
             def r4(n=n, s=s, rkey=rkey):
                 got(RD.at[n, 0], rkey, rkey + ("0",))
@@ -450,41 +490,44 @@
                     XG[n + CHUNKS, tp] = after
                 else:
                     OUT[k] = after
-                    pltpu.make_async_copy(OUT.at[k], out.at[pl.ds(k * ROWS, ROWS), :], hbm_sem.at[20 + k]).start()
-
+                    pltpu.make_async_copy(OUT.at[k], out.at[pl.ds(k * ROWS, ROWS), :], hbm_sem.at[24 + k]).start()
+
+            ua, ur = 2 * s * STAGE_GAP + k, (2 * s + 1) * STAGE_GAP + k
+            base = 0.01 * ua
             L, R, F, Dk = (akey + (r,) for r in "LRFD")
             extra = (("g", "L"), ("g", "R"), ("g", "F"), ("g", "D"))
-            sends = [("x+", BLOCK, L), ("x-", BLOCK, R), ("d", BLOCK, Dk)]
+            sends = [("x+", BLOCK, L, ua), ("x-", BLOCK, R, ua), ("d", BLOCK, Dk, ua)]
             waits = ("hbm",) if s == 0 else ()
             gsize = 8192
-            add = lambda *pairs: [(w, gsize, q) for w, q in pairs] if gains else []
+            add = lambda *pairs: [(w, gsize, q, -1) for w, q in pairs] if gains else []
             more = lambda q: (q,) if gains else ()
             a0_step = Step(a0, waits=waits, sends=sends + add(("x+", extra[0]), ("x-", extra[1]), ("d", extra[3])),
-                           rank=base + (0.0 if s else -1 + 0.1 * k), cost=0.1)
+                           rank=base + (0.0 if s else -1 + 0.1 * k))
             steps.append(a0_step)
             steps.append(Step(a1, waits=(L,) + more(extra[0]),
-                              sends=[("x+", BLOCK // 2, F), ("d", BLOCK, Dk)] + add(("x+", extra[2]), ("d", extra[3])), rank=base))
+                              sends=[("x+", BLOCK // 2, F, ua), ("d", BLOCK, Dk, ua)] + add(("x+", extra[2]), ("d", extra[3])), rank=base))
             steps.append(Step(a2, waits=(R,) + more(extra[1]),
-                              sends=[("x-", BLOCK // 2, F), ("d", BLOCK, Dk)] + add(("d", extra[3])), rank=base))
-            steps.append(Step(a3, waits=(F,) + more(extra[2]), sends=[("d", BLOCK, Dk)] + add(("d", extra[3])), rank=base))
+                              sends=[("x-", BLOCK // 2, F, ua), ("d", BLOCK, Dk, ua)] + add(("d", extra[3])), rank=base))
+            steps.append(Step(a3, waits=(F,) + more(extra[2]), sends=[("d", BLOCK, Dk, ua)] + add(("d", extra[3])), rank=base))
+            needs = ("gains",) if s == 0 and k else ()
+            steps.append(Step(normed, waits=(Dk,) + more(extra[3]), needs=needs, gives="gains" if gains else None,
+                              rank=2 + base, cost=COST["norm"]))
             if s == 1:
-                steps.append(Step(query_key, waits=(Dk,), needs=(("W", "qk"),), rank=2 + base, cost=2.0))
-                steps.append(Step(retained, needs=("tables",), rank=2 + base, cost=0.7))
-                end = ("W", "mx")
+                steps.append(Step(query_key, needs=(("W", "qk"), "tables"), rank=2 + base, cost=COST["qk"], gives=("kv", k)))
+                steps.append(Step(retained, needs=tuple(("kv", k - i) for i in range(half + 1)), rank=2 + base, cost=COST["ret"]))
+                end, cost = ("W", "mx"), COST["mx"]
             else:
-                needs = (("W", "gu"),) if gains else (("W", "gu"), "gains")
-                steps.append(Step(gate_up, waits=(Dk,) + more(extra[3]), needs=needs, rank=2 + base, cost=1.8,
-                                  gives="gains" if gains else None))
-                end = ("W", "dn")
+                steps.append(Step(gate_up, needs=(("W", "gu"),), rank=2 + base, cost=COST["gu"]))
+                end, cost = ("W", "dn"), COST["dn"]
             r = lambda q: rkey + (q,)
-            steps.append(Step(theirs, needs=(end,), rank=2 + base, cost=0.5,
-                              sends=[("d", BLOCK, r("2")), ("d", BLOCK, r("13")), ("d", BLOCK, r("13")), ("d", BLOCK, r("0"))]))
-            steps.append(Step(mine, rank=2 + base, cost=0.5))
-            steps.append(Step(r0, waits=(r("2"),), rank=base, sends=[("x+", BLOCK // 2, r("L")), ("x-", BLOCK // 2, r("R"))], cost=0.15))
-            steps.append(Step(r1, waits=(r("13"),), rank=base, sends=[("x+", BLOCK // 2, r("E")), ("x-", BLOCK // 2, r("E"))], cost=0.15))
-            steps.append(Step(r2, waits=(r("L"),), rank=base, sends=[("x+", BLOCK // 2, r("E"))]))
-            steps.append(Step(r3, waits=(r("R"),), rank=base, sends=[("x-", BLOCK // 2, r("E"))]))
-            steps.append(Step(r4, waits=(r("E"), r("0")), rank=base, cost=0.2))
+            steps.append(Step(theirs, needs=(end,), rank=2 + base, cost=cost,
+                              sends=[("d", BLOCK, r(q), ur) for q in ("2", "13", "13", "0")]))
+            steps.append(Step(mine, rank=2 + base, cost=cost))
+            steps.append(Step(r0, waits=(r("2"),), rank=base, sends=[("x+", BLOCK // 2, r("L"), ur), ("x-", BLOCK // 2, r("R"), ur)], cost=0.05))
+            steps.append(Step(r1, waits=(r("13"),), rank=base, sends=[("x+", BLOCK // 2, r("E"), ur), ("x-", BLOCK // 2, r("E"), ur)], cost=0.05))
+            steps.append(Step(r2, waits=(r("L"),), rank=base, sends=[("x+", BLOCK // 2, r("E"), ur)]))
+            steps.append(Step(r3, waits=(r("R"),), rank=base, sends=[("x-", BLOCK // 2, r("E"), ur)]))
+            steps.append(Step(r4, waits=(r("E"), r("0")), rank=base, cost=0.1))
         return steps
 
     for k in range(CHUNKS):
@@ -492,8 +535,14 @@
 
     order = in_order(lists)
     pl.semaphore_wait(barrier, 7)
-    for _, step in order:
-        step.run()
+    for _, step, which in order:
+        if which is None:
+            held.clear()
+            step.run()
+            step.held = list(held)
+            assert [w for w, _ in held] == [e[0] for e in step.sends]
+        else:
+            step.held[which][1]()
 
     for g in GROUPS:
         left(wspan(g, 15), ("w", g), ("w", g, "end"))
@@ -502,7 +551,7 @@
         left(XG.at[n, pl.ds(0, 7)], ("a", n), ("a", n, "D"))
         left(XG.at[n, pl.ds(0, 7)], ("r", n), ("r", n, "0"))
     for k in range(CHUNKS):
-        pltpu.make_async_copy(OUT.at[k], out.at[pl.ds(k * ROWS, ROWS), :], hbm_sem.at[20 + k]).wait()
+        pltpu.make_async_copy(OUT.at[k], out.at[pl.ds(k * ROWS, ROWS), :], hbm_sem.at[24 + k]).wait()
     assert len(recv.at) <= NSEM_RECV and len(sent.at) <= NSEM_SEND
 
 
@@ -516,14 +565,14 @@
     cos_t = jnp.asarray(np.cos(angles), F32)
     sin_t = jnp.asarray(np.sin(angles), F32)
     row = lambda v: v.reshape(1, -1)
-    small = [row(v) for v in (
-        gain_one, gain_mix, gain_two, scale_gate, scale_up, scale_down, scale_query, scale_key, scale_value,
-        scale_outgate, ret_gain, decay_rate, scale_mix,
-    )]
+    small = [
+        row(gain_one), row(gain_mix), row(gain_two), scale_gate, scale_up, row(scale_down), row(scale_query),
+        row(scale_key), row(scale_value), row(scale_outgate), row(ret_gain), decay_rate, row(scale_mix),
+    ]
     anywhere = pl.BlockSpec(memory_space=pl.ANY)
     vmem = pl.BlockSpec(memory_space=pltpu.VMEM)
     V = pltpu.VMEM
-    nine = 3 * CHUNKS
+    hops = 3 * CHUNKS
     return pl.pallas_call(
         layer_kernel,
         out_shape=jax.ShapeDtypeStruct((CHUNKS * ROWS, 256), BF16),
@@ -533,11 +582,12 @@
             V((2048, 768), BF16), V((384, 2048), BF16), V((2048, 1024), BF16), V((256, 2048), BF16),
             V((2, 128, 384), F32), V((384, 128), F32), V((4, 128, 256), F32), V((256, 128), F32),
             V((LEN, 256), F32), V((LEN, 256), F32), V((LEN, LEN), F32), V((8, 8, 256), F32),
-            V((nine, 8, ROWS, 256), BF16), V((ROWS, D), BF16), V((CHUNKS, ROWS, 384), BF16),
-            V((4, ROWS, 256), BF16), V((ROWS, 256), BF16), V((CHUNKS, 4, ROWS, 256), F32),
-            V((nine, 4, ROWS, 256), BF16), V((nine, 4, ROWS, 256), BF16), V((nine, 3, ROWS, 256), BF16),
-            V((nine, 2, 128, 256), BF16), V((nine, 2, ROWS, 256), BF16), V((CHUNKS, ROWS, 256), BF16),
-            pltpu.SemaphoreType.DMA((24,)), pltpu.SemaphoreType.DMA((NSEM_RECV,)), pltpu.SemaphoreType.DMA((NSEM_SEND,)),
+            V((hops, 8, ROWS, 256), BF16), V((CHUNKS, ROWS, D), BF16), V((CHUNKS, ROWS, 384), BF16),
+            V((CHUNKS, ROWS, 256), BF16), V((CHUNKS, ROWS, 256), BF16), V((CHUNKS * ROWS // LEN, LEN, 256), BF16),
+            V((CHUNKS * ROWS // LEN, LEN, 256), BF16), V((CHUNKS, ROWS, 256), BF16), V((CHUNKS, 4, ROWS, 256), F32),
+            V((hops, 4, ROWS, 256), BF16), V((hops, 4, ROWS, 256), BF16), V((hops, 3, ROWS, 256), BF16),
+            V((hops, 2, HALF, 256), BF16), V((hops, 2, ROWS, 256), BF16), V((CHUNKS, ROWS, 256), BF16),
+            pltpu.SemaphoreType.DMA((32,)), pltpu.SemaphoreType.DMA((NSEM_RECV,)), pltpu.SemaphoreType.DMA((NSEM_SEND,)),
         ],
         compiler_params=pltpu.CompilerParams(
             collective_id=0, has_side_effects=True, vmem_limit_bytes=60 * 1024 * 1024

time: 144 us -> 116 us (0.81)
  Pallas kernels: 139 us -> 113 us
  local copies, waits for them, and re-layouts: 3.72 us -> 1.77 us
    pallas_call x1, Pallas kernels: 139 us -> 113 us  [per_device(): pl.pallas_call(layer_kernel, out_shape=jax.ShapeDtypeStruct((CHUNKS * ROW...]
where the time goes in v2:
time: 116 us
  Pallas kernels  113 us (97%)
  local copies, waits for them, and re-layouts  1.77 us (2%)
    pallas_call x1, Pallas kernels, per_device(): pl.pallas_call(layer_kernel, out_shape=jax.ShapeDtypeStruct((CHUNKS * ROW...  113 us

profile of v2, /device:TPU:0, one launch (start us, length us, event | category | flops | bytes accessed | tf_op | source)
XLA Modules:
  0.0 115.8 jit_solution(12896313021188098247)
XLA Ops:
  0.7 113.4 %layer.1 = bf16[768,256]{1,0:T(8,128)(2,1)} custom-call(bf16[768,256]{1,0:T(8,128)(2,1)} %tokens.1, f32[128,384]{1,0:T(8,128)} %w_gate.1, f32[128,384]{1,0:T(8,128)} %w_up.1, f32[384,128]{1,0:T(8,128)} %w_down.1, f32[128,256]{1,0:T(8,128)} %w_query.1, f32[128,256]{1,0:T(8,128)} %w_key.1, f32[128,256]{1,0:T(8,128)} %w_value.1, f32[128,256]{1,0:T(8,128)} %w_outgate.1, ...), custom_call_target="tpu_custom_call" | custom-call | tf_op jit(solution)/shard_map/layer/pallas_call | solution.py:576
  114.1 1.8 %copy.27 = bf16[768,256]{1,0:T(8,128)(2,1)} copy(bf16[768,256]{1,0:T(8,128)(2,1)} %layer.1) | data formatting | bytes 786432

commit v3 on v2

--- a/solution.py
+++ b/solution.py
@@ -32,11 +32,14 @@
 
 
 START = 1.5
-MARGIN = 0.3
+MARGIN = 0.0
 LATENCY = 2.6
 WAYS = ("x+", "x-", "d", "y+", "y-", "z+", "z-")
-GROUP_GAP = 2.5
-STAGE_GAP = 10.0
+GROUP_BASE = (-1.25, 2.75, 8.25, 11.5)
+WPRI = (-0.75, -1.5, -9.25, -7.5, 1.75)
+XPRI = (-1.75, -1.0, -2.75, 2.0, 3.25, -4.0)
+RANKS = (11.25, -0.8)
+STAGE_GAP = 7.0
 COST = {"norm": 0.37, "gu": 0.73, "qk": 0.83, "ret": 0.4, "dn": 0.32, "mx": 0.25}
 GATE = (None, None, None)
 
@@ -114,8 +117,9 @@
         return self.ref.at[self.at[key]]
 
 
-NSEM_RECV = 288
-NSEM_SEND = 48
+NSEM_RECV = 156
+NSEM_SEND = 11
+NLOADS = 16
 
 
 def layer_kernel(
@@ -233,8 +237,8 @@
     lists.append(cast_steps)
 
     def weight_lists(order, g):
-        rank = 0.2 + 0.1 * order
-        base = GROUP_GAP * order
+        rank = RANKS[1] + 0.1 * order
+        base = GROUP_BASE[order]
         for half in (0, 1):
             a, b = ("y", "z") if half == 0 else ("z", "y")
 
@@ -249,7 +253,7 @@
                 def run():
                     for way in (b + "+", b + "-"):
                         send(wpart(g, at(i, 0), half), skey, key("s", i, way[1]), way)
-                return run, [(way, full, key("s", i, way[1]), base + (2 if i else 1.5)) for way in (b + "+", b + "-")]
+                return run, [(way, full, key("s", i, way[1]), base + WPRI[3 if i else 1]) for way in (b + "+", b + "-")]
 
             def own(half=half, at=at, a=a, b=b, key=key, full=full):
                 more, extra = both(0)
@@ -257,7 +261,7 @@
                     for way in (a + "+", a + "-"):
                         send(wpart(g, at(0, 0), half), skey, key("f", way[1]), way)
                     more()
-                return run, [(way, full, key("f", way[1]), base) for way in (a + "+", a + "-")] + extra
+                return run, [(way, full, key("f", way[1]), base + WPRI[0]) for way in (a + "+", a + "-")] + extra
 
             def first(side, half=half, at=at, a=a, b=b, key=key, full=full):
                 i, back, q = (3, "+", 0) if side == "+" else (1, "-", 1)
@@ -266,7 +270,7 @@
                     got(wpart(g, at(i, 0), half), skey, key("f", side))
                     send(wpart(g, at(i, 0), half, q), skey, key("f2"), a + back)
                     more()
-                return run, [(a + back, full // 2, key("f2"), base + 1)] + extra
+                return run, [(a + back, full // 2, key("f2"), base + WPRI[2])] + extra
 
             def far(half=half, at=at, a=a, b=b, key=key):
                 more, extra = both(2)
@@ -280,7 +284,7 @@
                 def run():
                     got(wpart(g, at(i, j), half), skey, key("s", i, side))
                     send(wpart(g, at(i, j), half, q), skey, ("w", g, "end"), b + back)
-                return run, [(b + back, full // 2, ("w", g, "end"), base + 3)]
+                return run, [(b + back, full // 2, ("w", g, "end"), base + WPRI[4])]
 
             run, sends = own()
             needs = [("cast", g)]
@@ -328,6 +332,7 @@
             n = s * CHUNKS + k
             xg = XG.at[n]
             akey, rkey = ("a", n), ("r", n)
+            acode, rcode, asend, rsend = ("a", k), ("r", k), ("as", s), ("rs", s)
 
             def slot(t, n=n):
                 return XG.at[n, t]
@@ -337,46 +342,46 @@
 
             gains = s == 0 and k == 0
 
-            def a0(s=s, akey=akey, slot=slot, gains=gains):
+            def a0(s=s, akey=acode, asend=asend, slot=slot, gains=gains):
                 if s == 0:
                     loads[("t", k)].wait()
                 for way, r in (("x+", "L"), ("x-", "R"), ("d", "D")):
-                    send(slot(tp), akey, akey + (r,), way)
+                    send(slot(tp), asend, akey + (r,), way)
                 if gains:
                     for i, gain in enumerate((gain_one, gain_mix, gain_two)):
                         GB[tp, i : i + 1, :] = gain[...]
                     for way, r in (("x+", "L"), ("x-", "R"), ("d", "D")):
                         send(GB.at[tp], ("g",), ("g", r), way)
 
-            def a1(akey=akey, slot=slot, half_of=half_of, gains=gains):
+            def a1(akey=acode, asend=asend, slot=slot, half_of=half_of, gains=gains):
                 t = tp_of(3, c)
-                got(slot(t), akey, akey + ("L",))
-                send(half_of(t, 0), akey, akey + ("F",), "x+")
-                send(slot(t), akey, akey + ("D",), "d")
+                got(slot(t), asend, akey + ("L",))
+                send(half_of(t, 0), asend, akey + ("F",), "x+")
+                send(slot(t), asend, akey + ("D",), "d")
                 if gains:
                     got(GB.at[t], ("g",), ("g", "L"))
                     send(GB.at[t], ("g",), ("g", "F"), "x+")
                     send(GB.at[t], ("g",), ("g", "D"), "d")
 
-            def a2(akey=akey, slot=slot, half_of=half_of, gains=gains):
+            def a2(akey=acode, asend=asend, slot=slot, half_of=half_of, gains=gains):
                 t = tp_of(1, c)
-                got(slot(t), akey, akey + ("R",))
-                send(half_of(t, 1), akey, akey + ("F",), "x-")
-                send(slot(t), akey, akey + ("D",), "d")
+                got(slot(t), asend, akey + ("R",))
+                send(half_of(t, 1), asend, akey + ("F",), "x-")
+                send(slot(t), asend, akey + ("D",), "d")
                 if gains:
                     got(GB.at[t], ("g",), ("g", "R"))
                     send(GB.at[t], ("g",), ("g", "D"), "d")
 
-            def a3(akey=akey, slot=slot, gains=gains):
+            def a3(akey=acode, asend=asend, slot=slot, gains=gains):
                 t = tp_of(2, c)
-                got(slot(t), akey, akey + ("F",))
-                send(slot(t), akey, akey + ("D",), "d")
+                got(slot(t), asend, akey + ("F",))
+                send(slot(t), asend, akey + ("D",), "d")
                 if gains:
                     got(GB.at[t], ("g",), ("g", "F"))
                     send(GB.at[t], ("g",), ("g", "D"), "d")
 
-            def normed(n=n, s=s, akey=akey, gains=gains):
-                got(XG.at[n, pl.ds(0, 4)], akey, akey + ("D",))
+            def normed(n=n, s=s, akey=acode, asend=asend, gains=gains):
+                got(XG.at[n, pl.ds(0, 4)], asend, akey + ("D",))
                 if gains:
                     got(GB.at[pl.ds(0, 4)], ("g",), ("g", "D"))
 
@@ -439,47 +444,47 @@
                     return jnp.dot(MX[k], W_mx[:, cols], preferred_element_type=F32)
                 return jnp.dot(HID[k], W_dn[:, cols], preferred_element_type=F32)
 
-            def theirs(n=n, rkey=rkey, product=product):
+            def theirs(n=n, rkey=rcode, rsend=rsend, product=product):
                 for i, r in ((2, "2"), (1, "13"), (3, "13"), (0, "0")):
                     PB[n, i] = product(i, 1 - c).astype(BF16)
-                    send(PB.at[n, i], rkey, rkey + (r,), "d", RD.at[n, i])
+                    send(PB.at[n, i], rsend, rkey + (r,), "d", RD.at[n, i])
 
             def mine(product=product):
                 for i in (2, 1, 3, 0):
                     OB[k, i] = product(i, c)
 
-            def r0(n=n, rkey=rkey):
-                got(RD.at[n, 2], rkey, rkey + ("2",))
+            def r0(n=n, rkey=rcode, rsend=rsend):
+                got(RD.at[n, 2], rsend, rkey + ("2",))
                 SB[n, 0] = (OB[k, 2] + RD[n, 2].astype(F32)).astype(BF16)
-                send(SB.at[n, 0, pl.ds(0, HALF)], rkey, rkey + ("L",), "x+", R1.at[n, 0])
-                send(SB.at[n, 0, pl.ds(HALF, HALF)], rkey, rkey + ("R",), "x-", R1.at[n, 1])
-
-            def r1(n=n, rkey=rkey):
-                got(RD.at[n, pl.ds(0, 2)], rkey, rkey + ("13",))
+                send(SB.at[n, 0, pl.ds(0, HALF)], rsend, rkey + ("L",), "x+", R1.at[n, 0])
+                send(SB.at[n, 0, pl.ds(HALF, HALF)], rsend, rkey + ("R",), "x-", R1.at[n, 1])
+
+            def r1(n=n, rkey=rcode, rsend=rsend):
+                got(RD.at[n, pl.ds(0, 2)], rsend, rkey + ("13",))
                 upper = OB[k, 1, HALF:ROWS] + RD[n, 1, HALF:ROWS].astype(F32)
                 SB[n, 1, HALF:ROWS] = upper.astype(BF16)
-                send(SB.at[n, 1, pl.ds(HALF, HALF)], rkey, rkey + ("E",), "x+", FIN.at[n, 0, pl.ds(HALF, HALF)])
+                send(SB.at[n, 1, pl.ds(HALF, HALF)], rsend, rkey + ("E",), "x+", FIN.at[n, 0, pl.ds(HALF, HALF)])
                 lower = OB[k, 3, 0:HALF] + RD[n, 3, 0:HALF].astype(F32)
                 SB[n, 2, 0:HALF] = lower.astype(BF16)
-                send(SB.at[n, 2, pl.ds(0, HALF)], rkey, rkey + ("E",), "x-", FIN.at[n, 1, pl.ds(0, HALF)])
-
-            def r2(n=n, rkey=rkey):
-                got(R1.at[n, 0], rkey, rkey + ("L",))
+                send(SB.at[n, 2, pl.ds(0, HALF)], rsend, rkey + ("E",), "x-", FIN.at[n, 1, pl.ds(0, HALF)])
+
+            def r2(n=n, rkey=rcode, rsend=rsend):
+                got(R1.at[n, 0], rsend, rkey + ("L",))
                 SB[n, 1, 0:HALF] = (
                     OB[k, 1, 0:HALF] + RD[n, 1, 0:HALF].astype(F32) + R1[n, 0].astype(F32)
                 ).astype(BF16)
-                send(SB.at[n, 1, pl.ds(0, HALF)], rkey, rkey + ("E",), "x+", FIN.at[n, 0, pl.ds(0, HALF)])
-
-            def r3(n=n, rkey=rkey):
-                got(R1.at[n, 1], rkey, rkey + ("R",))
+                send(SB.at[n, 1, pl.ds(0, HALF)], rsend, rkey + ("E",), "x+", FIN.at[n, 0, pl.ds(0, HALF)])
+
+            def r3(n=n, rkey=rcode, rsend=rsend):
+                got(R1.at[n, 1], rsend, rkey + ("R",))
                 SB[n, 2, HALF:ROWS] = (
                     OB[k, 3, HALF:ROWS] + RD[n, 3, HALF:ROWS].astype(F32) + R1[n, 1].astype(F32)
                 ).astype(BF16)
-                send(SB.at[n, 2, pl.ds(HALF, HALF)], rkey, rkey + ("E",), "x-", FIN.at[n, 1, pl.ds(HALF, HALF)])
-
-            def r4(n=n, s=s, rkey=rkey):
-                got(RD.at[n, 0], rkey, rkey + ("0",))
-                got(FIN.at[n], rkey, rkey + ("E",))
+                send(SB.at[n, 2, pl.ds(HALF, HALF)], rsend, rkey + ("E",), "x-", FIN.at[n, 1, pl.ds(HALF, HALF)])
+
+            def r4(n=n, s=s, rkey=rcode, rsend=rsend):
+                got(RD.at[n, 0], rsend, rkey + ("0",))
+                got(FIN.at[n], rsend, rkey + ("E",))
                 total = OB[k, 0] + RD[n, 0].astype(F32) + FIN[n, 0].astype(F32) + FIN[n, 1].astype(F32)
                 if s == 1:
                     total = total * s_mix[...]
@@ -489,14 +494,15 @@
                 if s < 2:
                     XG[n + CHUNKS, tp] = after
                 else:
-                    OUT[k] = after
-                    pltpu.make_async_copy(OUT.at[k], out.at[pl.ds(k * ROWS, ROWS), :], hbm_sem.at[24 + k]).start()
+                    OUT[k * ROWS : k * ROWS + ROWS, :] = after
+                    rows = pl.ds(k * ROWS, ROWS)
+                    pltpu.make_async_copy(OUT.at[rows, :], out.at[rows, :], hbm_sem.at[NLOADS]).start()
 
             ua, ur = 2 * s * STAGE_GAP + k, (2 * s + 1) * STAGE_GAP + k
             base = 0.01 * ua
             L, R, F, Dk = (akey + (r,) for r in "LRFD")
             extra = (("g", "L"), ("g", "R"), ("g", "F"), ("g", "D"))
-            sends = [("x+", BLOCK, L, ua), ("x-", BLOCK, R, ua), ("d", BLOCK, Dk, ua)]
+            sends = [("x+", BLOCK, L, ua + XPRI[0]), ("x-", BLOCK, R, ua + XPRI[0]), ("d", BLOCK, Dk, ua)]
             waits = ("hbm",) if s == 0 else ()
             gsize = 8192
             add = lambda *pairs: [(w, gsize, q, -1) for w, q in pairs] if gains else []
@@ -505,28 +511,28 @@
                            rank=base + (0.0 if s else -1 + 0.1 * k))
             steps.append(a0_step)
             steps.append(Step(a1, waits=(L,) + more(extra[0]),
-                              sends=[("x+", BLOCK // 2, F, ua), ("d", BLOCK, Dk, ua)] + add(("x+", extra[2]), ("d", extra[3])), rank=base))
+                              sends=[("x+", BLOCK // 2, F, ua + XPRI[1]), ("d", BLOCK, Dk, ua)] + add(("x+", extra[2]), ("d", extra[3])), rank=base))
             steps.append(Step(a2, waits=(R,) + more(extra[1]),
-                              sends=[("x-", BLOCK // 2, F, ua), ("d", BLOCK, Dk, ua)] + add(("d", extra[3])), rank=base))
+                              sends=[("x-", BLOCK // 2, F, ua + XPRI[1]), ("d", BLOCK, Dk, ua)] + add(("d", extra[3])), rank=base))
             steps.append(Step(a3, waits=(F,) + more(extra[2]), sends=[("d", BLOCK, Dk, ua)] + add(("d", extra[3])), rank=base))
             needs = ("gains",) if s == 0 and k else ()
             steps.append(Step(normed, waits=(Dk,) + more(extra[3]), needs=needs, gives="gains" if gains else None,
-                              rank=2 + base, cost=COST["norm"]))
+                              rank=RANKS[0] + base, cost=COST["norm"]))
             if s == 1:
-                steps.append(Step(query_key, needs=(("W", "qk"), "tables"), rank=2 + base, cost=COST["qk"], gives=("kv", k)))
-                steps.append(Step(retained, needs=tuple(("kv", k - i) for i in range(half + 1)), rank=2 + base, cost=COST["ret"]))
+                steps.append(Step(query_key, needs=(("W", "qk"), "tables"), rank=RANKS[0] + base, cost=COST["qk"], gives=("kv", k)))
+                steps.append(Step(retained, needs=tuple(("kv", k - i) for i in range(half + 1)), rank=RANKS[0] + base, cost=COST["ret"]))
                 end, cost = ("W", "mx"), COST["mx"]
             else:
-                steps.append(Step(gate_up, needs=(("W", "gu"),), rank=2 + base, cost=COST["gu"]))
+                steps.append(Step(gate_up, needs=(("W", "gu"),), rank=RANKS[0] + base, cost=COST["gu"]))
                 end, cost = ("W", "dn"), COST["dn"]
             r = lambda q: rkey + (q,)
-            steps.append(Step(theirs, needs=(end,), rank=2 + base, cost=cost,
+            steps.append(Step(theirs, needs=(end,), rank=RANKS[0] + base, cost=cost,
                               sends=[("d", BLOCK, r(q), ur) for q in ("2", "13", "13", "0")]))
-            steps.append(Step(mine, rank=2 + base, cost=cost))
-            steps.append(Step(r0, waits=(r("2"),), rank=base, sends=[("x+", BLOCK // 2, r("L"), ur), ("x-", BLOCK // 2, r("R"), ur)], cost=0.05))
-            steps.append(Step(r1, waits=(r("13"),), rank=base, sends=[("x+", BLOCK // 2, r("E"), ur), ("x-", BLOCK // 2, r("E"), ur)], cost=0.05))
-            steps.append(Step(r2, waits=(r("L"),), rank=base, sends=[("x+", BLOCK // 2, r("E"), ur)]))
-            steps.append(Step(r3, waits=(r("R"),), rank=base, sends=[("x-", BLOCK // 2, r("E"), ur)]))
+            steps.append(Step(mine, rank=RANKS[0] + base, cost=cost))
+            steps.append(Step(r0, waits=(r("2"),), rank=base, sends=[("x+", BLOCK // 2, r("L"), ur + XPRI[2]), ("x-", BLOCK // 2, r("R"), ur + XPRI[2])], cost=0.05))
+            steps.append(Step(r1, waits=(r("13"),), rank=base, sends=[(w, BLOCK // 2, r("E"), ur + XPRI[3]) for w in ("x+", "x-")], cost=0.05))
+            steps.append(Step(r2, waits=(r("L"),), rank=base, sends=[("x+", BLOCK // 2, r("E"), ur + XPRI[4])]))
+            steps.append(Step(r3, waits=(r("R"),), rank=base, sends=[("x-", BLOCK // 2, r("E"), ur + XPRI[4])]))
             steps.append(Step(r4, waits=(r("E"), r("0")), rank=base, cost=0.1))
         return steps
 
@@ -547,12 +553,11 @@
     for g in GROUPS:
         left(wspan(g, 15), ("w", g), ("w", g, "end"))
     left(GB.at[pl.ds(0, 7)], ("g",), ("g", "D"))
-    for n in range(3 * CHUNKS):
-        left(XG.at[n, pl.ds(0, 7)], ("a", n), ("a", n, "D"))
-        left(XG.at[n, pl.ds(0, 7)], ("r", n), ("r", n, "0"))
-    for k in range(CHUNKS):
-        pltpu.make_async_copy(OUT.at[k], out.at[pl.ds(k * ROWS, ROWS), :], hbm_sem.at[24 + k]).wait()
-    assert len(recv.at) <= NSEM_RECV and len(sent.at) <= NSEM_SEND
+    for s in range(3):
+        left(XG.at[pl.ds(0, CHUNKS), pl.ds(0, 7)], ("as", s), ("a", 0, "D"))
+        left(XG.at[pl.ds(0, CHUNKS), pl.ds(0, 7)], ("rs", s), ("r", 0, "0"))
+    pltpu.make_async_copy(OUT, out, hbm_sem.at[NLOADS]).wait()
+    assert len(recv.at) == NSEM_RECV and len(sent.at) == NSEM_SEND and len(loads) == NLOADS
 
 
 def per_device(
@@ -586,8 +591,8 @@
             V((CHUNKS, ROWS, 256), BF16), V((CHUNKS, ROWS, 256), BF16), V((CHUNKS * ROWS // LEN, LEN, 256), BF16),
             V((CHUNKS * ROWS // LEN, LEN, 256), BF16), V((CHUNKS, ROWS, 256), BF16), V((CHUNKS, 4, ROWS, 256), F32),
             V((hops, 4, ROWS, 256), BF16), V((hops, 4, ROWS, 256), BF16), V((hops, 3, ROWS, 256), BF16),
-            V((hops, 2, HALF, 256), BF16), V((hops, 2, ROWS, 256), BF16), V((CHUNKS, ROWS, 256), BF16),
-            pltpu.SemaphoreType.DMA((32,)), pltpu.SemaphoreType.DMA((NSEM_RECV,)), pltpu.SemaphoreType.DMA((NSEM_SEND,)),
+            V((hops, 2, HALF, 256), BF16), V((hops, 2, ROWS, 256), BF16), V((CHUNKS * ROWS, 256), BF16),
+            pltpu.SemaphoreType.DMA((NLOADS + 1,)), pltpu.SemaphoreType.DMA((NSEM_RECV,)), pltpu.SemaphoreType.DMA((NSEM_SEND,)),
         ],
         compiler_params=pltpu.CompilerParams(
             collective_id=0, has_side_effects=True, vmem_limit_bytes=60 * 1024 * 1024

time: 116 us -> 114 us (0.983)
  Pallas kernels: 113 us -> 111 us
    pallas_call x1, Pallas kernels: 113 us -> 111 us  [per_device(): pl.pallas_call(layer_kernel, out_shape=jax.ShapeDtypeStruct((CHUNKS * ROW...]
where the time goes in v3:
time: 114 us
  Pallas kernels  111 us (97%)
  local copies, waits for them, and re-layouts  1.77 us (2%)
    pallas_call x1, Pallas kernels, per_device(): pl.pallas_call(layer_kernel, out_shape=jax.ShapeDtypeStruct((CHUNKS * ROW...  111 us

profile of v3, /device:TPU:0, one launch (start us, length us, event | category | flops | bytes accessed | tf_op | source)
XLA Modules:
  0.0 113.7 jit_solution(9490913549430564440)
XLA Ops:
  0.7 111.3 %layer.1 = bf16[768,256]{1,0:T(8,128)(2,1)} custom-call(bf16[768,256]{1,0:T(8,128)(2,1)} %tokens.1, f32[128,384]{1,0:T(8,128)} %w_gate.1, f32[128,384]{1,0:T(8,128)} %w_up.1, f32[384,128]{1,0:T(8,128)} %w_down.1, f32[128,256]{1,0:T(8,128)} %w_query.1, f32[128,256]{1,0:T(8,128)} %w_key.1, f32[128,256]{1,0:T(8,128)} %w_value.1, f32[128,256]{1,0:T(8,128)} %w_outgate.1, ...), custom_call_target="tpu_custom_call" | custom-call | tf_op jit(solution)/shard_map/layer/pallas_call | solution.py:581
  111.9 1.8 %copy.27 = bf16[768,256]{1,0:T(8,128)(2,1)} copy(bf16[768,256]{1,0:T(8,128)(2,1)} %layer.1) | data formatting | bytes 786432

commit v4 on v3

--- a/solution.py
+++ b/solution.py
@@ -31,15 +31,16 @@
         self.needs, self.gives, self.cost, self.rank = needs, gives, cost, rank
 
 
-START = 1.5
-MARGIN = 0.0
+START = 0.7
+MARGIN = 0.1
 LATENCY = 2.6
+PARTNER = 1.7
 WAYS = ("x+", "x-", "d", "y+", "y-", "z+", "z-")
-GROUP_BASE = (-1.25, 2.75, 8.25, 11.5)
-WPRI = (-0.75, -1.5, -9.25, -7.5, 1.75)
-XPRI = (-1.75, -1.0, -2.75, 2.0, 3.25, -4.0)
-RANKS = (11.25, -0.8)
-STAGE_GAP = 7.0
+GROUP_BASE = (5.25, 5.75, 7.25, 9.25)
+WPRI = (-0.5, -1.0, -13.75, -2.5, 0.25)
+XPRI = (0.25, -3.75, 1.25, -1.0, 2.75, -11.5)
+RANKS = (26.5, 0.45)
+STAGE_GAP = 10.0
 COST = {"norm": 0.37, "gu": 0.73, "qk": 0.83, "ret": 0.4, "dn": 0.32, "mx": 0.25}
 GATE = (None, None, None)
 
@@ -50,7 +51,7 @@
 
 def in_order(lists):
     clock, free, given, order = 0.0, {}, set(), []
-    arrive = {"hbm": 0.5}
+    arrive = {"hbm": 0.3}
     for way in WAYS:
         free[way] = START
     pending = {way: [] for way in WAYS}
@@ -61,7 +62,7 @@
         _, _, size, key, step, which = entry
         done = max(free[way], clock) + link_time(way, size)
         free[way] = done
-        arrive[key] = max(arrive.get(key, 0.0), done + (0.9 if way == "d" else LATENCY))
+        arrive[key] = max(arrive.get(key, 0.0), done + (PARTNER if way == "d" else LATENCY))
         missing[key] -= 1
         order.append((clock, step, which))
 
@@ -117,9 +118,9 @@
         return self.ref.at[self.at[key]]
 
 
-NSEM_RECV = 156
+NSEM_RECV = 103
 NSEM_SEND = 11
-NLOADS = 16
+NLOADS = 11
 
 
 def layer_kernel(
@@ -129,7 +130,7 @@
     out,
     W_gu, W_dn, W_qk, W_mx,
     F_gu, F_dn, F_qk, F_mx,
-    COS, SIN, DEC, GB, XG, NX, HID, QB, OG, KB, VB, MX, OB, PB, RD, SB, R1, FIN, OUT,
+    TURN, DEC, GB, XG, NX, HID, QB, OG, KB, VB, MX, OB, PB, RD, SB, R1, FIN, OUT,
     hbm_sem, recv_sem, send_sem,
 ):
     fs, tp = lax.axis_index("fs"), lax.axis_index("tp")
@@ -176,16 +177,19 @@
         loads[key] = pltpu.make_async_copy(src, dst, hbm_sem.at[len(loads)])
         loads[key].start()
 
-    load("g", w_gate, F_gu.at[0])
-    load("u", w_up, F_gu.at[1])
+    def load_all(key, sources, dst):
+        at = len(loads)
+        loads[key] = pltpu.make_async_copy(dst, dst, hbm_sem.at[at])
+        for n, src in enumerate(sources):
+            pltpu.make_async_copy(src, dst.at[n], hbm_sem.at[at]).start()
+
+    load_all("gu", (w_gate, w_up), F_gu)
     for k in range(CHUNKS):
         load(("t", k), tokens.at[pl.ds(k * ROWS, ROWS), :], XG.at[k, tp])
     load("d", w_down, F_dn)
-    for n, w in enumerate((w_query, w_key, w_value, w_outgate)):
-        load(("q", n), w, F_qk.at[n])
+    load_all("q", (w_query, w_key, w_value, w_outgate), F_qk)
     load("m", w_mix, F_mx)
-    load("cos", cos_t, COS)
-    load("sin", sin_t, SIN)
+    load_all("turn", (cos_t, sin_t), TURN)
 
     barrier = pltpu.get_barrier_semaphore()
     for way in WAYS:
@@ -209,8 +213,7 @@
         return W[g].at[:, pl.ds(0, 128 * pieces)]
 
     def cast_gu():
-        loads["g"].wait()
-        loads["u"].wait()
+        loads["gu"].wait()
         rows = pl.ds(pl.multiple_of(fs * 128, 128), 128)
         for j in range(3):
             W_gu[rows, 256 * j : 256 * j + 128] = F_gu[0, :, 128 * j : 128 * j + 128].astype(BF16)
@@ -222,8 +225,8 @@
 
     def cast_qk():
         rows = pl.ds(pl.multiple_of(fs * 128, 128), 128)
+        loads["q"].wait()
         for n in range(4):
-            loads[("q", n)].wait()
             W_qk[rows, 256 * n : 256 * n + 256] = F_qk[n].astype(BF16)
 
     def cast_mx():
@@ -252,25 +255,26 @@
             def both(i, half=half, at=at, a=a, b=b, key=key, full=full):
                 def run():
                     for way in (b + "+", b + "-"):
-                        send(wpart(g, at(i, 0), half), skey, key("s", i, way[1]), way)
-                return run, [(way, full, key("s", i, way[1]), base + WPRI[3 if i else 1]) for way in (b + "+", b + "-")]
+                        send(wpart(g, at(i, 0), half), skey, key("s", i), way)
+                return run, [(way, full, key("s", i), base + WPRI[3 if i else 1]) for way in (b + "+", b + "-")]
 
             def own(half=half, at=at, a=a, b=b, key=key, full=full):
                 more, extra = both(0)
                 def run():
                     for way in (a + "+", a + "-"):
-                        send(wpart(g, at(0, 0), half), skey, key("f", way[1]), way)
+                        send(wpart(g, at(0, 0), half), skey, key("f"), way)
                     more()
-                return run, [(way, full, key("f", way[1]), base + WPRI[0]) for way in (a + "+", a + "-")] + extra
-
-            def first(side, half=half, at=at, a=a, b=b, key=key, full=full):
-                i, back, q = (3, "+", 0) if side == "+" else (1, "-", 1)
-                more, extra = both(i)
+                return run, [(way, full, key("f"), base + WPRI[0]) for way in (a + "+", a + "-")] + extra
+
+            def first(half=half, at=at, a=a, b=b, key=key, full=full):
+                (one, extra_one), (two, extra_two) = both(3), both(1)
                 def run():
-                    got(wpart(g, at(i, 0), half), skey, key("f", side))
-                    send(wpart(g, at(i, 0), half, q), skey, key("f2"), a + back)
-                    more()
-                return run, [(a + back, full // 2, key("f2"), base + WPRI[2])] + extra
+                    got(wspan(g, 1), skey, key("f"))
+                    for i, back, q in ((3, "+", 0), (1, "-", 1)):
+                        send(wpart(g, at(i, 0), half, q), skey, key("f2"), a + back)
+                    one()
+                    two()
+                return run, [(a + back, full // 2, key("f2"), base + WPRI[2]) for back in "+-"] + extra_one + extra_two
 
             def far(half=half, at=at, a=a, b=b, key=key):
                 more, extra = both(2)
@@ -279,30 +283,27 @@
                     more()
                 return run, extra
 
-            def second(i, side, half=half, at=at, a=a, b=b, key=key, full=full):
-                j, back, q = (3, "+", 0) if side == "+" else (1, "-", 1)
+            def second(i, half=half, at=at, a=a, b=b, key=key, full=full):
                 def run():
-                    got(wpart(g, at(i, j), half), skey, key("s", i, side))
-                    send(wpart(g, at(i, j), half, q), skey, ("w", g, "end"), b + back)
-                return run, [(b + back, full // 2, ("w", g, "end"), base + WPRI[4])]
+                    got(wspan(g, 1), skey, key("s", i))
+                    for j, back, q in ((3, "+", 0), (1, "-", 1)):
+                        send(wpart(g, at(i, j), half, q), skey, ("w", g, "end"), b + back)
+                return run, [(b + back, full // 2, ("w", g, "end"), base + WPRI[4]) for back in "+-"]
 
             run, sends = own()
             needs = [("cast", g)]
             if order and GATE[order - 1]:
                 needs += [(GATE[order - 1], GROUPS[order - 1], h) for h in (0, 1)]
             steps = [Step(run, sends=sends, needs=needs, gives=("own", g, half), rank=rank)]
-            for side in ("+", "-"):
-                run, sends = first(side)
-                steps.append(Step(run, waits=(key("f", side),), sends=sends, rank=rank,
-                                  gives=("near", g, half) if side == "-" else None))
+            run, sends = first()
+            steps.append(Step(run, waits=(key("f"),), sends=sends, rank=rank, gives=("near", g, half)))
             run, sends = far()
             steps.append(Step(run, waits=(key("f2"),), sends=sends, rank=rank, gives=("far", g, half)))
             lists.append(steps)
             steps = []
             for i in (0, 3, 1, 2):
-                for side in ("+", "-"):
-                    run, sends = second(i, side)
-                    steps.append(Step(run, waits=(key("s", i, side),), sends=sends, rank=rank))
+                run, sends = second(i)
+                steps.append(Step(run, waits=(key("s", i),), sends=sends, rank=rank))
             steps[-1].gives = ("last", g, half)
             lists.append(steps)
 
@@ -314,8 +315,7 @@
         weight_lists(order, g)
 
     def tables():
-        loads["cos"].wait()
-        loads["sin"].wait()
+        loads["turn"].wait()
         n = lax.broadcasted_iota(jnp.int32, (LEN, LEN), 0)
         m = lax.broadcasted_iota(jnp.int32, (LEN, LEN), 1)
         distance = jnp.maximum(n - m, 0).astype(F32)
@@ -345,32 +345,26 @@
             def a0(s=s, akey=acode, asend=asend, slot=slot, gains=gains):
                 if s == 0:
                     loads[("t", k)].wait()
-                for way, r in (("x+", "L"), ("x-", "R"), ("d", "D")):
+                for way, r in (("x+", "L"), ("x-", "L"), ("d", "D")):
                     send(slot(tp), asend, akey + (r,), way)
                 if gains:
                     for i, gain in enumerate((gain_one, gain_mix, gain_two)):
                         GB[tp, i : i + 1, :] = gain[...]
-                    for way, r in (("x+", "L"), ("x-", "R"), ("d", "D")):
+                    for way, r in (("x+", "L"), ("x-", "L"), ("d", "D")):
                         send(GB.at[tp], ("g",), ("g", r), way)
 
-            def a1(akey=acode, asend=asend, slot=slot, half_of=half_of, gains=gains):
-                t = tp_of(3, c)
-                got(slot(t), asend, akey + ("L",))
-                send(half_of(t, 0), asend, akey + ("F",), "x+")
-                send(slot(t), asend, akey + ("D",), "d")
+            def a1(akey=acode, asend=asend, slot=slot, half_of=half_of, n=n, gains=gains):
+                got(XG.at[n, pl.ds(0, 2)], asend, akey + ("L",))
+                before, after = tp_of(3, c), tp_of(1, c)
+                send(half_of(before, 0), asend, akey + ("F",), "x+")
+                send(half_of(after, 1), asend, akey + ("F",), "x-")
+                send(slot(before), asend, akey + ("D",), "d")
+                send(slot(after), asend, akey + ("D",), "d")
                 if gains:
-                    got(GB.at[t], ("g",), ("g", "L"))
-                    send(GB.at[t], ("g",), ("g", "F"), "x+")
-                    send(GB.at[t], ("g",), ("g", "D"), "d")
-
-            def a2(akey=acode, asend=asend, slot=slot, half_of=half_of, gains=gains):
-                t = tp_of(1, c)
-                got(slot(t), asend, akey + ("R",))
-                send(half_of(t, 1), asend, akey + ("F",), "x-")
-                send(slot(t), asend, akey + ("D",), "d")
-                if gains:
-                    got(GB.at[t], ("g",), ("g", "R"))
-                    send(GB.at[t], ("g",), ("g", "D"), "d")
+                    got(GB.at[pl.ds(0, 2)], ("g",), ("g", "L"))
+                    send(GB.at[before], ("g",), ("g", "F"), "x+")
+                    send(GB.at[before], ("g",), ("g", "D"), "d")
+                    send(GB.at[after], ("g",), ("g", "D"), "d")
 
             def a3(akey=acode, asend=asend, slot=slot, gains=gains):
                 t = tp_of(2, c)
@@ -410,7 +404,7 @@
                 at = slice(ROWS * half, ROWS * half + ROWS)
                 even = lax.broadcasted_iota(jnp.int32, (ROWS, 256), 1) % 2 == 0
                 swapped = jnp.where(even, -pltpu.roll(v, 255, 1), pltpu.roll(v, 1, 1))
-                return (v * COS[at, :] + swapped * SIN[at, :]).astype(BF16)
+                return (v * TURN[0, at, :] + swapped * TURN[1, at, :]).astype(BF16)
 
             def query_key():
                 at = slice(ROWS * half, ROWS * half + ROWS)
@@ -457,7 +451,7 @@
                 got(RD.at[n, 2], rsend, rkey + ("2",))
                 SB[n, 0] = (OB[k, 2] + RD[n, 2].astype(F32)).astype(BF16)
                 send(SB.at[n, 0, pl.ds(0, HALF)], rsend, rkey + ("L",), "x+", R1.at[n, 0])
-                send(SB.at[n, 0, pl.ds(HALF, HALF)], rsend, rkey + ("R",), "x-", R1.at[n, 1])
+                send(SB.at[n, 0, pl.ds(HALF, HALF)], rsend, rkey + ("L",), "x-", R1.at[n, 1])
 
             def r1(n=n, rkey=rcode, rsend=rsend):
                 got(RD.at[n, pl.ds(0, 2)], rsend, rkey + ("13",))
@@ -469,14 +463,11 @@
                 send(SB.at[n, 2, pl.ds(0, HALF)], rsend, rkey + ("E",), "x-", FIN.at[n, 1, pl.ds(0, HALF)])
 
             def r2(n=n, rkey=rcode, rsend=rsend):
-                got(R1.at[n, 0], rsend, rkey + ("L",))
+                got(R1.at[n], rsend, rkey + ("L",))
                 SB[n, 1, 0:HALF] = (
                     OB[k, 1, 0:HALF] + RD[n, 1, 0:HALF].astype(F32) + R1[n, 0].astype(F32)
                 ).astype(BF16)
                 send(SB.at[n, 1, pl.ds(0, HALF)], rsend, rkey + ("E",), "x+", FIN.at[n, 0, pl.ds(0, HALF)])
-
-            def r3(n=n, rkey=rcode, rsend=rsend):
-                got(R1.at[n, 1], rsend, rkey + ("R",))
                 SB[n, 2, HALF:ROWS] = (
                     OB[k, 3, HALF:ROWS] + RD[n, 3, HALF:ROWS].astype(F32) + R1[n, 1].astype(F32)
                 ).astype(BF16)
@@ -500,23 +491,19 @@
 
             ua, ur = 2 * s * STAGE_GAP + k, (2 * s + 1) * STAGE_GAP + k
             base = 0.01 * ua
-            L, R, F, Dk = (akey + (r,) for r in "LRFD")
-            extra = (("g", "L"), ("g", "R"), ("g", "F"), ("g", "D"))
-            sends = [("x+", BLOCK, L, ua + XPRI[0]), ("x-", BLOCK, R, ua + XPRI[0]), ("d", BLOCK, Dk, ua)]
+            L, F, Dk = (akey + (r,) for r in "LFD")
+            extra = {r: ("g", r) for r in "LFD"}
+            sends = [("x+", BLOCK, L, ua + XPRI[0]), ("x-", BLOCK, L, ua + XPRI[0]), ("d", BLOCK, Dk, ua)]
             waits = ("hbm",) if s == 0 else ()
-            gsize = 8192
-            add = lambda *pairs: [(w, gsize, q, -1) for w, q in pairs] if gains else []
-            more = lambda q: (q,) if gains else ()
-            a0_step = Step(a0, waits=waits, sends=sends + add(("x+", extra[0]), ("x-", extra[1]), ("d", extra[3])),
-                           rank=base + (0.0 if s else -1 + 0.1 * k))
-            steps.append(a0_step)
-            steps.append(Step(a1, waits=(L,) + more(extra[0]),
-                              sends=[("x+", BLOCK // 2, F, ua + XPRI[1]), ("d", BLOCK, Dk, ua)] + add(("x+", extra[2]), ("d", extra[3])), rank=base))
-            steps.append(Step(a2, waits=(R,) + more(extra[1]),
-                              sends=[("x-", BLOCK // 2, F, ua + XPRI[1]), ("d", BLOCK, Dk, ua)] + add(("d", extra[3])), rank=base))
-            steps.append(Step(a3, waits=(F,) + more(extra[2]), sends=[("d", BLOCK, Dk, ua)] + add(("d", extra[3])), rank=base))
+            add = lambda *pairs: [(w, 8192, extra[q], -9) for w, q in pairs] if gains else []
+            more = lambda q: (extra[q],) if gains else ()
+            steps.append(Step(a0, waits=waits, sends=sends + add(("x+", "L"), ("x-", "L"), ("d", "D")),
+                              rank=base + (0.0 if s else -1 + 0.1 * k)))
+            sends = [("x+", BLOCK // 2, F, ua + XPRI[1]), ("x-", BLOCK // 2, F, ua + XPRI[1])] + 2 * [("d", BLOCK, Dk, ua)]
+            steps.append(Step(a1, waits=(L,) + more("L"), sends=sends + add(("x+", "F"), ("d", "D"), ("d", "D")), rank=base))
+            steps.append(Step(a3, waits=(F,) + more("F"), sends=[("d", BLOCK, Dk, ua)] + add(("d", "D")), rank=base))
             needs = ("gains",) if s == 0 and k else ()
-            steps.append(Step(normed, waits=(Dk,) + more(extra[3]), needs=needs, gives="gains" if gains else None,
+            steps.append(Step(normed, waits=(Dk,) + more("D"), needs=needs, gives="gains" if gains else None,
                               rank=RANKS[0] + base, cost=COST["norm"]))
             if s == 1:
                 steps.append(Step(query_key, needs=(("W", "qk"), "tables"), rank=RANKS[0] + base, cost=COST["qk"], gives=("kv", k)))
@@ -529,10 +516,10 @@
             steps.append(Step(theirs, needs=(end,), rank=RANKS[0] + base, cost=cost,
                               sends=[("d", BLOCK, r(q), ur) for q in ("2", "13", "13", "0")]))
             steps.append(Step(mine, rank=RANKS[0] + base, cost=cost))
-            steps.append(Step(r0, waits=(r("2"),), rank=base, sends=[("x+", BLOCK // 2, r("L"), ur + XPRI[2]), ("x-", BLOCK // 2, r("R"), ur + XPRI[2])], cost=0.05))
-            steps.append(Step(r1, waits=(r("13"),), rank=base, sends=[(w, BLOCK // 2, r("E"), ur + XPRI[3]) for w in ("x+", "x-")], cost=0.05))
-            steps.append(Step(r2, waits=(r("L"),), rank=base, sends=[("x+", BLOCK // 2, r("E"), ur + XPRI[4])]))
-            steps.append(Step(r3, waits=(r("R"),), rank=base, sends=[("x-", BLOCK // 2, r("E"), ur + XPRI[4])]))
+            two = lambda q, i: [(w, BLOCK // 2, r(q), ur + XPRI[i]) for w in ("x+", "x-")]
+            steps.append(Step(r0, waits=(r("2"),), rank=base, sends=two("L", 2), cost=0.03))
+            steps.append(Step(r1, waits=(r("13"),), rank=base, sends=two("E", 3), cost=0.03))
+            steps.append(Step(r2, waits=(r("L"),), rank=base, sends=two("E", 4), cost=0.05))
             steps.append(Step(r4, waits=(r("E"), r("0")), rank=base, cost=0.1))
         return steps
 
@@ -586,7 +573,7 @@
         scratch_shapes=[
             V((2048, 768), BF16), V((384, 2048), BF16), V((2048, 1024), BF16), V((256, 2048), BF16),
             V((2, 128, 384), F32), V((384, 128), F32), V((4, 128, 256), F32), V((256, 128), F32),
-            V((LEN, 256), F32), V((LEN, 256), F32), V((LEN, LEN), F32), V((8, 8, 256), F32),
+            V((2, LEN, 256), F32), V((LEN, LEN), F32), V((8, 8, 256), F32),
             V((hops, 8, ROWS, 256), BF16), V((CHUNKS, ROWS, D), BF16), V((CHUNKS, ROWS, 384), BF16),
             V((CHUNKS, ROWS, 256), BF16), V((CHUNKS, ROWS, 256), BF16), V((CHUNKS * ROWS // LEN, LEN, 256), BF16),
             V((CHUNKS * ROWS // LEN, LEN, 256), BF16), V((CHUNKS, ROWS, 256), BF16), V((CHUNKS, 4, ROWS, 256), F32),

time: 114 us -> 114 us (level)
  no operation moved by 1% of the time
where the time goes in v4:
time: 114 us
  Pallas kernels  111 us (97%)
  local copies, waits for them, and re-layouts  1.77 us (2%)
    pallas_call x1, Pallas kernels, per_device(): pl.pallas_call(layer_kernel, out_shape=jax.ShapeDtypeStruct((CHUNKS * ROW...  111 us

profile of v4, /device:TPU:0, one launch (start us, length us, event | category | flops | bytes accessed | tf_op | source)
XLA Modules:
  0.0 113.5 jit_solution(15215021715142034614)
XLA Ops:
  0.7 111.1 %layer.1 = bf16[768,256]{1,0:T(8,128)(2,1)} custom-call(bf16[768,256]{1,0:T(8,128)(2,1)} %tokens.1, f32[128,384]{1,0:T(8,128)} %w_gate.1, f32[128,384]{1,0:T(8,128)} %w_up.1, f32[384,128]{1,0:T(8,128)} %w_down.1, f32[128,256]{1,0:T(8,128)} %w_query.1, f32[128,256]{1,0:T(8,128)} %w_key.1, f32[128,256]{1,0:T(8,128)} %w_value.1, f32[128,256]{1,0:T(8,128)} %w_outgate.1, ...), custom_call_target="tpu_custom_call" | custom-call | tf_op jit(solution)/shard_map/layer/pallas_call | solution.py:568
  111.8 1.8 %copy.27 = bf16[768,256]{1,0:T(8,128)(2,1)} copy(bf16[768,256]{1,0:T(8,128)(2,1)} %layer.1) | data formatting | bytes 786432

commit v5 on v4

--- a/solution.py
+++ b/solution.py
@@ -390,7 +390,7 @@
                         NX[k, r, 256 * t : 256 * t + 256] = (hs[t] * scale * GB[t, s : s + 1, :]).astype(BF16)
                     return carry
 
-                lax.fori_loop(0, ROWS // 16, rows_of, 0, unroll=4)
+                lax.fori_loop(0, ROWS // 16, rows_of, 0, unroll=8)
 
             def gate_up():
                 for j in range(3):

time: 114 us -> 113 us (level)
  no operation moved by 1% of the time
where the time goes in v5:
time: 113 us
  Pallas kernels  111 us (98%)
  local copies, waits for them, and re-layouts  1.77 us (2%)
    pallas_call x1, Pallas kernels, per_device(): pl.pallas_call(layer_kernel, out_shape=jax.ShapeDtypeStruct((CHUNKS * ROW...  111 us

profile of v5, /device:TPU:0, one launch (start us, length us, event | category | flops | bytes accessed | tf_op | source)
XLA Modules:
  0.0 113.3 jit_solution(11218300949504271908)
XLA Ops:
  0.7 110.8 %layer.1 = bf16[768,256]{1,0:T(8,128)(2,1)} custom-call(bf16[768,256]{1,0:T(8,128)(2,1)} %tokens.1, f32[128,384]{1,0:T(8,128)} %w_gate.1, f32[128,384]{1,0:T(8,128)} %w_up.1, f32[384,128]{1,0:T(8,128)} %w_down.1, f32[128,256]{1,0:T(8,128)} %w_query.1, f32[128,256]{1,0:T(8,128)} %w_key.1, f32[128,256]{1,0:T(8,128)} %w_value.1, f32[128,256]{1,0:T(8,128)} %w_outgate.1, ...), custom_call_target="tpu_custom_call" | custom-call | tf_op jit(solution)/shard_map/layer/pallas_call | solution.py:568
  111.5 1.8 %copy.27 = bf16[768,256]{1,0:T(8,128)(2,1)} copy(bf16[768,256]{1,0:T(8,128)(2,1)} %layer.1) | data formatting | bytes 786432
